TPU v7x, 32 devices: a whole 2x2x4 slice. The times are simulated.
32 devices in a mesh: fs: 4 (over y, x), tp: 8 (over z, core).
Axes of the slice: x: 2, y: 2, z: 4, core: 2. Of those that a mesh axis runs over, the one named last changes fastest.
Arguments:
- value_input: bfloat16 [8192, 2048], P('fs', 'tp'), may hold values from -50 to 50
- value_cotangent: bfloat16 [8192, 512], P('fs'), may hold values from -6 to 6
- value_factor: bfloat16 [512, 128], replicated, may hold values from -10 to 10
- value_master: float32 [512, 2048], P('fs', 'tp'), may hold values from -0.125 to 0.125
- value_first: float32 [128, 2048], P('fs', 'tp'), may hold values from -4 to 4
- value_second: float32 [128, 2048], P('fs', 'tp'), may hold values from 0.01 to 0.2
- mixed_heads: bfloat16 [8192, 1024], P('fs', 'tp'), may hold values from -6 to 6
- output_cotangent: bfloat16 [8192, 2048], P('fs', 'tp'), may hold values from -50 to 50
- output_factor: bfloat16 [1024, 128], replicated, may hold values from -10 to 10
- output_master: float32 [1024, 2048], P('fs', 'tp'), may hold values from -0.1875 to 0.1875
- output_first: float32 [128, 2048], P('fs', 'tp'), may hold values from -4 to 4
- output_second: float32 [128, 2048], P('fs', 'tp'), may hold values from 0.01 to 0.2
Outputs:
- value_step: float32 [512, 2048], P('fs', 'tp')
- value_new_master: float32 [512, 2048], P('fs', 'tp')
- value_copy: bfloat16 [512, 2048], P(None, 'tp')
- value_first_new: float32 [128, 2048], P('fs', 'tp')
- value_second_new: float32 [128, 2048], P('fs', 'tp')
- output_step: float32 [1024, 2048], P('fs', 'tp')
- output_new_master: float32 [1024, 2048], P('fs', 'tp')
- output_copy: bfloat16 [1024, 2048], P(None, 'tp')
- output_first_new: float32 [128, 2048], P('fs', 'tp')
- output_second_new: float32 [128, 2048], P('fs', 'tp')
All inputs are finite; a program needn't handle non-finite values.
Results may differ from a plain program's by a relative error of at most 0.001.
Values may be sent and summed in bfloat16 or wider, within the bound.
A program may use at most 64 MiB of HBM per device.

v0:
```python
import functools

import jax
import jax.numpy as jnp
from jax import lax
from jax.experimental import pallas as pl
from jax.experimental.pallas import tpu as pltpu
from jax.sharding import PartitionSpec as P

MESH = pl.DeviceIdType.MESH
ANY = pl.BlockSpec(memory_space=pl.ANY)
HBM = pl.BlockSpec(memory_space=pltpu.HBM)
VMEM = pl.BlockSpec(memory_space=pltpu.VMEM)
BF16 = jnp.bfloat16
F32 = jnp.float32


def split(wide, axis):
    high = wide.astype(BF16)
    low = (wide - high.astype(F32)).astype(BF16)
    return jnp.concatenate([high, low], axis=axis)


def gather_kernel(
    fs, tp, pair,
    vin, vcot, vfac, vmas, vm1, vm2, heads, ocot, ofac, omas, om1, om2,
    v_all, o_all, v1_all, v2_all, o1_all, o2_all, vm_all, om_all, totals,
    vfac_v, ofac_v, vin_v, vcot_v, heads_v, ocot_v, v1_v, v2_v, o1_v, o2_v, vm_v, om_v,
    heads_in, images, partial, partial_in, band_v, first_sums, second_sums,
    load_sem, own_sem, put_sem, heads_send, heads_recv, image_send, image_recv, relay_send,
    rs_send, rs_recv, all_send, all_recv, s1_send, s1_recv, s2_send, s2_recv, pre_send, pre_recv,
):
    f = lax.axis_index("fs")
    t = lax.axis_index("tp")
    rank = vfac.shape[1]
    band = rank // fs
    tokens, width = heads.shape
    block = tokens // tp
    columns = vin.shape[1]

    def fs_peer(j):
        return lax.rem(f + j, fs)

    def tp_peer(j):
        return lax.rem(t + j, tp)

    sources = (heads, om1, om2, vm1, vm2, vcot, vin, omas, vmas, ocot, vfac, ofac)
    places = (heads_v, o1_v, o2_v, v1_v, v2_v, vcot_v, vin_v, om_v, vm_v, ocot_v, vfac_v, ofac_v)
    loads = [
        pltpu.make_async_copy(a, b, load_sem.at[i]) for i, (a, b) in enumerate(zip(sources, places))
    ]
    for load in loads:
        load.start()

    barrier = pltpu.get_barrier_semaphore()
    for j in range(1, tp):
        pl.semaphore_signal(barrier, inc=1, device_id={"tp": tp_peer(j)}, device_id_type=MESH)
    for j in range(1, fs):
        pl.semaphore_signal(barrier, inc=1, device_id={"fs": fs_peer(j)}, device_id_type=MESH)
    pl.semaphore_wait(barrier, tp + fs - 2)

    sent = []

    def send(src, dst, send_sem, recv_sem, where):
        copy = pltpu.make_async_remote_copy(
            src_ref=src, dst_ref=dst, send_sem=send_sem, recv_sem=recv_sem,
            device_id=where, device_id_type=MESH,
        )
        copy.start()
        sent.append(copy)

    def landed(dst, send_sem, recv_sem, where):
        pltpu.make_async_remote_copy(
            src_ref=dst, dst_ref=dst, send_sem=send_sem, recv_sem=recv_sem,
            device_id=where, device_id_type=MESH,
        ).wait_recv()

    loads[0].wait()
    for j in range(1, tp):
        d = tp_peer(j)
        send(
            heads_v.at[pl.ds(pl.multiple_of(d * block, block), block)], heads_in.at[t],
            heads_send.at[j], heads_recv.at[t], {"tp": d},
        )
    own_heads = pltpu.make_async_copy(
        heads_v.at[pl.ds(pl.multiple_of(t * block, block), block)], heads_in.at[t], own_sem
    )
    own_heads.start()

    puts = []

    def prefetch(i, load, local, whole):
        load.wait()
        rows = local.shape[0]
        here = whole.at[pl.ds(pl.multiple_of(f * rows, rows), rows)]
        for j in range(1, fs):
            d = fs_peer(j)
            send(local, here, pre_send.at[i, j], pre_recv.at[i, f], {"fs": d})
        put = pltpu.make_async_copy(local, here, put_sem.at[i])
        put.start()
        puts.append(put)

    prefetch(0, loads[1], o1_v, o1_all)
    prefetch(1, loads[2], o2_v, o2_all)
    prefetch(2, loads[3], v1_v, v1_all)
    prefetch(3, loads[4], v2_v, v2_all)

    loads[5].wait()
    loads[6].wait()
    loads[10].wait()
    total = jnp.zeros((2 * rank, columns), F32)
    step = 256 if tokens % 256 == 0 else tokens
    for i in range(tokens // step):
        rows = pl.ds(i * step, step)
        image = jnp.dot(vcot_v[rows, :], vfac_v[...], preferred_element_type=F32)
        total = total + lax.dot_general(
            split(image, 1), vin_v[rows, :], (((0,), (0,)), ((), ())), preferred_element_type=F32
        )

    def scatter(k, total):
        partial[k] = (total[:rank] + total[rank:]).reshape(fs, band, columns)
        for j in range(1, fs):
            d = fs_peer(j)
            send(partial.at[k, d], partial_in.at[k, f], rs_send.at[k, j], rs_recv.at[k, f], {"fs": d})

    def reduce(k, whole):
        mine = partial[k, f]
        for j in range(1, fs):
            d = fs_peer(j)
            landed(partial_in.at[k, d], rs_send.at[k, j], rs_recv.at[k, d], {"fs": d})
            mine = mine + partial_in[k, d]
        band_v[k] = mine
        first_sums[k, f] = jnp.full((8, 128), jnp.sum(mine * mine), F32)
        for j in range(1, fs):
            d = fs_peer(j)
            send(first_sums.at[k, f], first_sums.at[k, f], s1_send.at[k, j], s1_recv.at[k, f], {"fs": d})
        for j in range(1, fs):
            d = fs_peer(j)
            send(band_v.at[k], whole.at[f], all_send.at[k, j], all_recv.at[k, f], {"fs": d})
        put = pltpu.make_async_copy(band_v.at[k], whole.at[f], put_sem.at[6 + k])
        put.start()
        puts.append(put)

    def sums_on(k):
        mine = first_sums[k, f]
        for j in range(1, fs):
            d = fs_peer(j)
            landed(first_sums.at[k, d], s1_send.at[k, j], s1_recv.at[k, d], {"fs": d})
            mine = mine + first_sums[k, d]
        second_sums[k, t] = mine
        for j in range(1, tp):
            d = tp_peer(j)
            send(second_sums.at[k, t], second_sums.at[k, t], s2_send.at[k, j], s2_recv.at[k, t], {"tp": d})

    def sums_end(k):
        mine = second_sums[k, t]
        for j in range(1, tp):
            d = tp_peer(j)
            landed(second_sums.at[k, d], s2_send.at[k, j], s2_recv.at[k, d], {"tp": d})
            mine = mine + second_sums[k, d]
        totals[k] = mine

    scatter(0, total)
    prefetch(4, loads[7], om_v, om_all)
    prefetch(5, loads[8], vm_v, vm_all)

    own_heads.wait()
    loads[11].wait()

    def image_term(s):
        return jnp.dot(
            heads_in[s], ofac_v[pl.ds(pl.multiple_of(s * width, width), width), :],
            preferred_element_type=F32,
        )

    image = image_term(t)
    for j in range(1, tp):
        d = tp_peer(j)
        landed(heads_in.at[d], heads_send.at[j], heads_recv.at[d], {"tp": d})
        image = image + image_term(d)
    images[t] = image.T

    chip = t // pair
    core = t % pair
    chips = tp // pair

    def give(d, j):
        send(images.at[t], images.at[t], image_send.at[j], image_recv.at[t], {"tp": d})

    for j in range(1, chips):
        give(lax.rem(chip + j, chips) * pair + core, j - 1)
    for j in range(1, pair):
        give(chip * pair + lax.rem(core + j, pair), chips - 2 + j)

    loads[9].wait()

    def term(s):
        return jnp.dot(
            split(images[s], 0), ocot_v[pl.ds(pl.multiple_of(s * block, block), block), :],
            preferred_element_type=F32,
        )

    total = term(t)
    reduce(0, v_all)

    def arrived(s):
        landed(images.at[s], image_send.at[0], image_recv.at[s], {"tp": s})

    for j in range(1, pair):
        s = chip * pair + lax.rem(core + j, pair)
        arrived(s)
        total = total + term(s)
    for j in range(1, chips):
        s = lax.rem(chip + j, chips) * pair + core
        arrived(s)
        for i in range(1, pair):
            send(
                images.at[s], images.at[s], relay_send.at[(j - 1) * (pair - 1) + i - 1],
                image_recv.at[s], {"tp": chip * pair + lax.rem(core + i, pair)},
            )
        total = total + term(s)
    for j in range(1, chips):
        for i in range(1, pair):
            s = lax.rem(chip + j, chips) * pair + lax.rem(core + i, pair)
            arrived(s)
            total = total + term(s)

    scatter(1, total)
    sums_on(0)
    reduce(1, o_all)
    sums_on(1)
    sums_end(0)
    sums_end(1)

    for k, whole in ((0, v_all), (1, o_all)):
        for j in range(1, fs):
            d = fs_peer(j)
            landed(whole.at[d], all_send.at[k, j], all_recv.at[k, d], {"fs": d})
    for i, (local, whole) in enumerate(
        ((o1_v, o1_all), (o2_v, o2_all), (v1_v, v1_all), (v2_v, v2_all), (om_v, om_all), (vm_v, vm_all))
    ):
        rows = local.shape[0]
        for j in range(1, fs):
            d = fs_peer(j)
            there = whole.at[pl.ds(pl.multiple_of(d * rows, rows), rows)]
            landed(there, pre_send.at[i, j], pre_recv.at[i, d], {"fs": d})
    for copy in sent:
        copy.wait_send()
    for put in puts:
        put.wait()


def finish_kernel(
    fs, tp,
    v_all, o_all, v1_all, v2_all, o1_all, o2_all, vm_all, om_all, totals, vfac, ofac,
    v_step, v_new, v_copy, v_first, v_second, o_step, o_new, o_copy, o_first, o_second,
):
    f = lax.axis_index("fs")

    def one(k, proj, first, second, master, factor, step_out, new_out, copy_out, first_out, second_out):
        rank, columns = proj.shape
        scale = lax.rsqrt(totals[k, 0:1, 0:1] / (rank * columns * tp) + 1e-06)

        def moments(rows):
            scaled = scale * proj[rows, :]
            first_new = 0.9 * first[rows, :] + 0.1 * scaled
            second_new = 0.95 * second[rows, :] + 0.05 * scaled * scaled
            return first_new, second_new

        band = rank // fs
        first_own, second_own = moments(pl.ds(pl.multiple_of(f * band, band), band))
        first_out[...] = first_own
        second_out[...] = second_own
        first_new, second_new = moments(pl.ds(0, rank))
        direction = split(first_new / (jnp.sqrt(second_new) + 1e-08), 0)

        def step_of(rows):
            left = factor[rows, :]
            return jnp.dot(
                jnp.concatenate([left, left], axis=1), direction, preferred_element_type=F32
            )

        count = step_out.shape[0]
        own = pl.ds(pl.multiple_of(f * count, count), count)
        step = step_of(own)
        step_out[...] = step
        new_out[...] = master[own, :] - 0.002 * step
        for i in range(fs):
            rows = pl.ds(i * count, count)
            copy_out[rows, :] = (master[rows, :] - 0.002 * step_of(rows)).astype(BF16)

    one(0, v_all, v1_all, v2_all, vm_all, vfac, v_step, v_new, v_copy, v_first, v_second)
    one(1, o_all, o1_all, o2_all, om_all, ofac, o_step, o_new, o_copy, o_first, o_second)


def on_device(vin, vcot, vfac, vmas, vm1, vm2, heads, ocot, ofac, omas, om1, om2):
    fs = lax.axis_size("fs")
    tp = lax.axis_size("tp")
    pair = 2 if tp % 2 == 0 else 1
    rank = vfac.shape[1]
    band = rank // fs
    columns = vin.shape[1]
    tokens, width = heads.shape
    block = tokens // tp

    def like(array):
        return pltpu.VMEM(array.shape, array.dtype)

    def shape(*dims):
        return jax.ShapeDtypeStruct(dims, F32)

    dma = pltpu.SemaphoreType.DMA
    gathered = pl.pallas_call(
        functools.partial(gather_kernel, fs, tp, pair),
        out_shape=(
            shape(fs, band, columns), shape(fs, band, columns),
            shape(rank, columns), shape(rank, columns), shape(rank, columns), shape(rank, columns),
            shape(fs * vmas.shape[0], columns), shape(fs * omas.shape[0], columns),
            shape(2, 8, 128),
        ),
        in_specs=[HBM] * 12,
        out_specs=(ANY,) * 8 + (VMEM,),
        scratch_shapes=[
            like(vfac), like(ofac), like(vin), like(vcot), like(heads), like(ocot), like(vm1), like(vm2), like(om1), like(om2),
            like(vmas), like(omas),
            pltpu.VMEM((tp, block, width), BF16),
            pltpu.VMEM((tp, rank, block), F32),
            pltpu.VMEM((2, fs, band, columns), F32),
            pltpu.VMEM((2, fs, band, columns), F32),
            pltpu.VMEM((2, band, columns), F32),
            pltpu.VMEM((2, fs, 8, 128), F32),
            pltpu.VMEM((2, tp, 8, 128), F32),
            dma((12,)), dma, dma((8,)), dma((tp,)), dma((tp,)), dma((tp,)), dma((tp,)), dma((tp,)),
            dma((2, fs)), dma((2, fs)), dma((2, fs)), dma((2, fs)), dma((2, fs)), dma((2, fs)),
            dma((2, tp)), dma((2, tp)), dma((6, fs)), dma((6, fs)),
        ],
        compiler_params=pltpu.CompilerParams(
            collective_id=0, has_side_effects=True, vmem_limit_bytes=60 * 1024 * 1024
        ),
    )(vin, vcot, vfac, vmas, vm1, vm2, heads, ocot, ofac, omas, om1, om2)
    v_all, o_all, v1_all, v2_all, o1_all, o2_all, vm_all, om_all, totals = gathered
    v_all = v_all.reshape(rank, columns)
    o_all = o_all.reshape(rank, columns)

    def out(array, rows, kind=F32):
        return jax.ShapeDtypeStruct((rows, columns), kind)

    return pl.pallas_call(
        functools.partial(finish_kernel, fs, tp),
        out_shape=(
            out(vmas, vmas.shape[0]), out(vmas, vmas.shape[0]), out(vmas, fs * vmas.shape[0], BF16),
            out(vm1, band), out(vm1, band),
            out(omas, omas.shape[0]), out(omas, omas.shape[0]), out(omas, fs * omas.shape[0], BF16),
            out(om1, band), out(om1, band),
        ),
        in_specs=[VMEM] * 11,
        out_specs=(VMEM,) * 10,
        compiler_params=pltpu.CompilerParams(vmem_limit_bytes=60 * 1024 * 1024),
    )(v_all, o_all, v1_all, v2_all, o1_all, o2_all, vm_all, om_all, totals, vfac, ofac)


def solution(mesh):
    both = P("fs", "tp")
    in_specs = (both, P("fs", None), P(), both, both, both, both, both, P(), both, both, both)
    out_specs = (
        both, both, P(None, "tp"), both, both, both, both, P(None, "tp"), both, both,
    )
    return jax.shard_map(
        on_device, mesh=mesh, in_specs=in_specs, out_specs=out_specs, check_vma=False
    )
```

profile of v0, /device:TPU:0, one launch (start us, length us, event | category | flops | bytes accessed | tf_op | source)
XLA Modules:
  0.0 50.1 jit_solution(7196001077757040056)
XLA Ops:
  0.6 46.2 %shard_map.195 = (f32[4,32,256]{2,1,0:T(8,128)}, f32[4,32,256]{2,1,0:T(8,128)}, f32[128,256]{1,0:T(8,128)}, f32[128,256]{1,0:T(8,128)}, f32[128,256]{1,0:T(8,128...) custom-call(bf16[2048,256]{1,0:T(8,128)(2,1)} %vin.1, ...), custom_call_target="tpu_custom_call" | custom-call | tf_op jit(solution)/shard_map/pallas_call | solution.py:313
  46.9 3.3 %shard_map.196 = (f32[128,256]{1,0:T(8,128)}, f32[128,256]{1,0:T(8,128)}, bf16[512,256]{1,0:T(8,128)(2,1)}, f32[32,256]{1,0:T(8,128)}, f32[32,256]{1,0:T(8,128)}...) custom-call(f32[128,256]{1,0:T(8,128)} %bitcast.2, ...), custom_call_target="tpu_custom_call" | custom-call | tf_op jit(solution)/shard_map/pallas_call | solution.py:348
where the time goes:
time: 50.3 us; the launch traced here: 50.1 us
  Pallas kernels  49.5 us (98%)
  between operations  0.65 us (1%)
    pallas_call x1, Pallas kernels, on_device(): pl.pallas_call(functools.partial(gather_kernel, fs, tp, pair), out_shape=...  46.2 us
    pallas_call x1, Pallas kernels, on_device(): pl.pallas_call(functools.partial(finish_kernel, fs, tp), out_shape=(out(v...  3.26 us

commit v1 on v0

v1 whole, which is shorter than its diff:
```python
import functools

import jax
import jax.numpy as jnp
from jax import lax
from jax.experimental import pallas as pl
from jax.experimental.pallas import tpu as pltpu
from jax.sharding import PartitionSpec as P

MESH = pl.DeviceIdType.MESH
ANY = pl.BlockSpec(memory_space=pl.ANY)
HBM = pl.BlockSpec(memory_space=pltpu.HBM)
VMEM = pl.BlockSpec(memory_space=pltpu.VMEM)
BF16 = jnp.bfloat16
F32 = jnp.float32
HOP = 4
POWER = 15
PEAK = 256.0
SCALE_ROWS = 16
PIECES = 4


def split(wide, axis):
    high = wide.astype(BF16)
    low = (wide - high.astype(F32)).astype(BF16)
    return jnp.concatenate([high, low], axis=axis)


def encode(x):
    top = jnp.max(jnp.abs(x), axis=0, keepdims=True)
    top = jnp.maximum(top * 1.01, 1e-30).astype(BF16)
    u = x * (PEAK / top.astype(F32))
    u3 = u * u * u
    u5 = u3 * u * u
    return (u5 * u5 * u5).astype(BF16), jnp.broadcast_to(top, (SCALE_ROWS, x.shape[1]))


def decode(ref, rows):
    y = ref[:rows, :].astype(F32)
    top = ref[rows:, :].astype(F32)[0:1, :]
    size = jnp.abs(y)
    root = jnp.exp(jnp.log(jnp.maximum(size, 1e-37)) * (1.0 / POWER))
    root = jnp.where(size < 2e-37, 0.0, root) * (top * (1.0 / PEAK))
    return jnp.where(y < 0.0, -root, root)


def gather_kernel(
    fs, tp,
    vin, vcot, vfac, vmas, vm1, vm2, heads, ocot, ofac, omas, om1, om2,
    o_all, o1_all, o2_all, om_all, totals, v_step, v_new, v_copy, v_first, v_second,
    vfac_v, ofac_v, vin_v, vcot_v, heads_v, heads_in, ocot_v, ocot_in, v1_v, v2_v, vm_v,
    own_v, left_v, right_v, pre_in, pre_out, suf_in, suf_out, acc_own, acc_pair, pair_out, pair_in,
    partial, partial_in, band_v, dir_all, first_sums, second_sums, all_sums,
    load_sem, heads_send, heads_recv, ocot_send, ocot_recv, pre_send, pre_recv, suf_send, suf_recv,
    pair_send, pair_recv, rs_send, rs_recv, all_send, all_recv, s1_send, s1_recv, s2_send, s2_recv,
    so_send, so_recv, mom_send, mom_recv, mas_send, mas_recv, copy_send, copy_recv,
):
    f = lax.axis_index("fs")
    t = lax.axis_index("tp")
    chip = t // 2
    core = t % 2
    chips = tp // 2
    last = chips - 1
    partner = {"tp": chip * 2 + (1 - core)}
    rank = vfac.shape[1]
    band = rank // fs
    tokens, width = heads.shape
    columns = vin.shape[1]
    half = tokens // 2
    blocks, _, block = own_v.shape
    mine_at = pl.multiple_of(core * half, half)
    pair_at = pl.multiple_of((1 - core) * half, half)

    def fs_peer(j):
        return lax.rem(f + j, fs)

    def tp_peer(j):
        return lax.rem(t + j, tp)

    def own_rows(ref):
        rows = ref.shape[0] // fs
        return ref.at[pl.ds(pl.multiple_of(f * rows, rows), rows)]

    jobs = [
        (heads.at[pl.ds(pair_at, half)], heads_v.at[pl.ds(pair_at, half)]),
        (ofac, ofac_v),
        (heads.at[pl.ds(mine_at, half)], heads_v.at[pl.ds(mine_at, half)]),
        (om1, own_rows(o1_all)), (om2, own_rows(o2_all)),
        (vfac, vfac_v), (vcot, vcot_v), (vin, vin_v),
        (ocot.at[pl.ds(pair_at, half)], ocot_v.at[pl.ds(pair_at, half)]),
        (ocot.at[pl.ds(mine_at, half)], ocot_v.at[pl.ds(mine_at, half)]),
        (omas, own_rows(om_all)),
        (vmas, vm_v), (vm1, v1_v), (vm2, v2_v),
    ]
    loads = [pltpu.make_async_copy(a, b, load_sem.at[i]) for i, (a, b) in enumerate(jobs)]
    for load in loads:
        load.start()

    barrier = pltpu.get_barrier_semaphore()
    for j in range(1, tp):
        pl.semaphore_signal(barrier, inc=1, device_id={"tp": tp_peer(j)}, device_id_type=MESH)
    for j in range(1, fs):
        pl.semaphore_signal(barrier, inc=1, device_id={"fs": fs_peer(j)}, device_id_type=MESH)
    pl.semaphore_wait(barrier, tp + fs - 2)

    sent = []

    def remote(src, dst, send_sem, recv_sem, where):
        return pltpu.make_async_remote_copy(
            src_ref=src, dst_ref=dst, send_sem=send_sem, recv_sem=recv_sem,
            device_id=where, device_id_type=MESH,
        )

    def send(src, dst, send_sem, recv_sem, where):
        copy = remote(src, dst, send_sem, recv_sem, where)
        copy.start()
        sent.append(copy)

    def landed(dst, send_sem, recv_sem, where):
        remote(dst, dst, send_sem, recv_sem, where).wait_recv()

    loads[0].wait()
    send(heads_v.at[pl.ds(pair_at, half)], heads_in, heads_send, heads_recv, partner)
    for i, whole in ((0, o1_all), (1, o2_all)):
        loads[3 + i].wait()
        here = own_rows(whole)
        for j in range(1, fs):
            send(here, here, mom_send.at[i, j], mom_recv.at[i, f], {"fs": fs_peer(j)})

    loads[5].wait()
    loads[6].wait()
    loads[7].wait()
    total = jnp.zeros((2 * rank, columns), F32)
    stride = 256 if tokens % 256 == 0 else tokens
    for i in range(tokens // stride):
        rows = pl.ds(i * stride, stride)
        image = jnp.dot(vcot_v[rows, :], vfac_v[...], preferred_element_type=F32)
        total = total + lax.dot_general(
            split(image, 1), vin_v[rows, :], (((0,), (0,)), ((), ())), preferred_element_type=F32
        )

    def scatter(k, whole):
        partial[k] = whole.reshape(fs, band, columns)
        for j in range(1, fs):
            d = fs_peer(j)
            send(partial.at[k, d], partial_in.at[k, f], rs_send.at[k, j], rs_recv.at[k, f], {"fs": d})

    def reduce(k):
        mine = partial[k, f]
        for j in range(1, fs):
            d = fs_peer(j)
            landed(partial_in.at[k, d], rs_send.at[k, j], rs_recv.at[k, d], {"fs": d})
            mine = mine + partial_in[k, d]
        return mine

    scatter(0, total[:rank] + total[rank:])

    loads[8].wait()
    send(ocot_v.at[pl.ds(pair_at, half)], ocot_in, ocot_send, ocot_recv, partner)

    loads[1].wait()
    loads[2].wait()

    def factor_of(s):
        rows = ofac_v[pl.ds(pl.multiple_of(s * width, width), width), :]
        return rows.astype(F32).T.astype(BF16)

    def against(left, right):
        return lax.dot_general(left, right, (((1,), (1,)), ((), ())), preferred_element_type=F32)

    factor_mine = factor_of(t)
    factor_pair = factor_of(chip * 2 + (1 - core))
    landed(heads_in, heads_send, heads_recv, partner)
    for k in range(blocks):
        here = heads_v[pl.ds(pl.multiple_of(mine_at + k * block, block), block), :]
        own_v[k] = against(factor_mine, here) + against(factor_pair, heads_in[pl.ds(k * block, block), :])
    acc_own[...] = jnp.zeros_like(acc_own)
    acc_pair[...] = jnp.zeros_like(acc_pair)
    loads[9].wait()
    landed(ocot_in, ocot_send, ocot_recv, partner)

    def to_right(k):
        return remote(pre_out.at[k], pre_in.at[k], pre_send.at[k], pre_recv.at[k], {"tp": lax.rem(t + 2, tp)})

    def to_left(k):
        return remote(suf_out.at[k], suf_in.at[k], suf_send.at[k], suf_recv.at[k], {"tp": lax.rem(t + tp - 2, tp)})

    def pack(ref, x):
        coded, top = encode(x)
        ref[:rank, :] = coded
        ref[rank:, :] = top

    def step(i, _):
        k = i - HOP * chip

        @pl.when((k >= 0) & (k < blocks))
        def _():
            @pl.when(chip > 0)
            def _():
                to_right(k).wait_recv()
                left_v[k] = decode(pre_in.at[k], rank)

            @pl.when(chip == 0)
            def _():
                left_v[k] = jnp.zeros((rank, block), F32)

            @pl.when(chip < last)
            def _():
                pack(pre_out.at[k], left_v[k] + own_v[k])
                to_right(k).start()

        m = i - HOP * (last - chip)

        @pl.when((m >= 0) & (m < blocks))
        def _():
            @pl.when(chip < last)
            def _():
                to_left(m).wait_recv()
                right_v[m] = decode(suf_in.at[m], rank)

            @pl.when(chip == last)
            def _():
                right_v[m] = jnp.zeros((rank, block), F32)

            @pl.when(chip > 0)
            def _():
                pack(suf_out.at[m], right_v[m] + own_v[m])
                to_left(m).start()

        n = i - HOP * jnp.maximum(chip, last - chip)

        @pl.when((n >= 0) & (n < blocks))
        def _():
            two = split(left_v[n] + own_v[n] + right_v[n], 0)
            here = pl.ds(pl.multiple_of(mine_at + n * block, block), block)
            there = pl.ds(pl.multiple_of(n * block, block), block)
            acc_own[...] += jnp.dot(two, ocot_v[here, :], preferred_element_type=F32)
            acc_pair[...] += jnp.dot(two, ocot_in[there, :], preferred_element_type=F32)

        return 0

    masters = own_rows(om_all)
    piece = masters.shape[0] // PIECES

    def send_masters(i):
        if i == 0:
            loads[10].wait()
        here = masters.at[pl.ds(i * piece, piece)]
        for j in range(1, fs):
            send(here, here, mas_send.at[i, j], mas_recv.at[i, f], {"fs": fs_peer(j)})

    def value_sums():
        mine = reduce(0)
        band_v[0] = mine
        first_sums[f] = jnp.full((1, 128), jnp.sum(mine * mine), F32)
        for j in range(1, fs):
            send(first_sums.at[f], first_sums.at[f], s1_send.at[j], s1_recv.at[f], {"fs": fs_peer(j)})

    def value_sums_on():
        mine = first_sums[f]
        for j in range(1, fs):
            d = fs_peer(j)
            landed(first_sums.at[d], s1_send.at[j], s1_recv.at[d], {"fs": d})
            mine = mine + first_sums[d]
        second_sums[t] = mine
        for j in range(1, tp):
            send(second_sums.at[t], second_sums.at[t], s2_send.at[j], s2_recv.at[t], {"tp": tp_peer(j)})

    def value_direction():
        mine = second_sums[t]
        for j in range(1, tp):
            d = tp_peer(j)
            landed(second_sums.at[d], s2_send.at[j], s2_recv.at[d], {"tp": d})
            mine = mine + second_sums[d]
        scale = lax.rsqrt(mine[0:1, 0:1] / (rank * columns * tp) + 1e-06)
        for i in (12, 13):
            loads[i].wait()
        scaled = scale * band_v[0]
        first_new = 0.9 * v1_v[...] + 0.1 * scaled
        second_new = 0.95 * v2_v[...] + 0.05 * scaled * scaled
        v_first[...] = first_new
        v_second[...] = second_new
        dir_all[f] = first_new / (jnp.sqrt(second_new) + 1e-08)
        for j in range(1, fs):
            send(dir_all.at[f], dir_all.at[f], all_send.at[0, j], all_recv.at[0, f], {"fs": fs_peer(j)})

    def value_finish():
        for j in range(1, fs):
            d = fs_peer(j)
            landed(dir_all.at[d], all_send.at[0, j], all_recv.at[0, d], {"fs": d})
        direction = split(dir_all[...].reshape(rank, columns), 0)
        count = v_step.shape[0]
        left = vfac_v[pl.ds(pl.multiple_of(f * count, count), count), :]
        move = jnp.dot(jnp.concatenate([left, left], axis=1), direction, preferred_element_type=F32)
        loads[11].wait()
        fresh = vm_v[...] - 0.002 * move
        v_step[...] = move
        v_new[...] = fresh
        here = own_rows(v_copy)
        here[...] = fresh.astype(BF16)
        for j in range(1, fs):
            send(here, here, copy_send.at[j], copy_recv.at[f], {"fs": fs_peer(j)})

    steps = blocks + HOP * last
    events = [(0, functools.partial(send_masters, 0))]
    plan = (
        (4, functools.partial(send_masters, 1)), (6, value_sums), (8, functools.partial(send_masters, 2)),
        (10, value_sums_on), (12, functools.partial(send_masters, 3)), (16, value_direction),
    )
    done = 0
    for at, event in events + list(plan):
        at = min(at, steps)
        if at > done:
            lax.fori_loop(done, at, step, 0)
            done = at
        event()
    lax.fori_loop(done, steps, step, 0)

    pair_out[...] = acc_pair[:rank, :] + acc_pair[rank:, :]
    send(pair_out, pair_in, pair_send, pair_recv, partner)
    mine = acc_own[:rank, :] + acc_own[rank:, :]
    landed(pair_in, pair_send, pair_recv, partner)
    scatter(1, mine + pair_in[...])

    value_finish()

    mine = reduce(1)
    o_all[f] = mine
    me = f * tp + t
    count = fs * tp
    all_sums[me] = jnp.full((1, 128), jnp.sum(mine * mine), F32)

    def spread(j):
        d = lax.rem(me + j, count)
        return remote(all_sums.at[me], all_sums.at[me], so_send.at[j], so_recv.at[me], {"fs": d // tp, "tp": d % tp})

    def spread_start(j, _):
        spread(j).start()
        return 0

    lax.fori_loop(1, count, spread_start, 0)
    for j in range(1, fs):
        send(o_all.at[f], o_all.at[f], all_send.at[1, j], all_recv.at[1, f], {"fs": fs_peer(j)})

    for j in range(1, fs):
        d = fs_peer(j)
        landed(o_all.at[d], all_send.at[1, j], all_recv.at[1, d], {"fs": d})
        for i, whole in ((0, o1_all), (1, o2_all)):
            there = whole.at[pl.ds(pl.multiple_of(d * band, band), band)]
            landed(there, mom_send.at[i, j], mom_recv.at[i, d], {"fs": d})
        for i in range(PIECES):
            there = om_all.at[pl.ds(pl.multiple_of(d * PIECES * piece + i * piece, piece), piece)]
            landed(there, mas_send.at[i, j], mas_recv.at[i, d], {"fs": d})
        rows = v_step.shape[0]
        there = v_copy.at[pl.ds(pl.multiple_of(d * rows, rows), rows)]
        landed(there, copy_send.at[j], copy_recv.at[d], {"fs": d})

    def spread_end(j, _):
        d = lax.rem(me + j, count)
        remote(all_sums.at[d], all_sums.at[d], so_send.at[j], so_recv.at[d], {"fs": d // tp, "tp": d % tp}).wait_recv()
        spread(j).wait_send()
        return 0

    lax.fori_loop(1, count, spread_end, 0)
    totals[...] = jnp.sum(all_sums[...], axis=0)

    def drain(k, _):
        @pl.when(chip < last)
        def _():
            to_right(k).wait_send()

        @pl.when(chip > 0)
        def _():
            to_left(k).wait_send()

        return 0

    lax.fori_loop(0, blocks, drain, 0)
    for copy in sent:
        copy.wait_send()


def finish_kernel(
    fs, tp,
    o_all, o1_all, o2_all, om_all, totals, ofac, v_step, v_new, v_copy, v_first, v_second,
    v_step_out, v_new_out, v_copy_out, v_first_out, v_second_out,
    o_step_out, o_new_out, o_copy_out, o_first_out, o_second_out,
    step_v, new_v, copy_v, first_v, second_v, out_sem,
):
    f = lax.axis_index("fs")
    puts = []

    def put(src, dst):
        copy = pltpu.make_async_copy(src, dst, out_sem.at[len(puts)])
        copy.start()
        puts.append(copy)

    for src, dst in (
        (v_step, v_step_out), (v_new, v_new_out), (v_copy, v_copy_out), (v_first, v_first_out), (v_second, v_second_out),
    ):
        put(src, dst)
    rank, columns = o1_all.shape
    band = rank // fs
    scale = lax.rsqrt(totals[0:1, 0:1] / (rank * columns * tp) + 1e-06)

    def moments(proj, rows):
        scaled = scale * proj
        first_new = 0.9 * o1_all[rows, :] + 0.1 * scaled
        second_new = 0.95 * o2_all[rows, :] + 0.05 * scaled * scaled
        return first_new, second_new

    first_v[...], second_v[...] = moments(o_all[f], pl.ds(pl.multiple_of(f * band, band), band))
    put(first_v, o_first_out)
    put(second_v, o_second_out)
    first_new, second_new = moments(o_all[...].reshape(rank, columns), pl.ds(0, rank))
    direction = split(first_new / (jnp.sqrt(second_new) + 1e-08), 0)

    def step_of(rows):
        left = ofac[rows, :]
        return jnp.dot(jnp.concatenate([left, left], axis=1), direction, preferred_element_type=F32)

    count = step_v.shape[0]
    own = pl.ds(pl.multiple_of(f * count, count), count)
    move = step_of(own)
    step_v[...] = move
    put(step_v, o_step_out)
    new_v[...] = om_all[own, :] - 0.002 * move
    put(new_v, o_new_out)
    for i in range(fs):
        rows = pl.ds(i * count, count)
        copy_v[rows, :] = (om_all[rows, :] - 0.002 * step_of(rows)).astype(BF16)
        put(copy_v.at[rows], o_copy_out.at[rows])
    for copy in puts:
        copy.wait()


def on_device(vin, vcot, vfac, vmas, vm1, vm2, heads, ocot, ofac, omas, om1, om2):
    fs = lax.axis_size("fs")
    tp = lax.axis_size("tp")
    rank = vfac.shape[1]
    band = rank // fs
    columns = vin.shape[1]
    tokens, width = heads.shape
    half = tokens // 2
    block = 128 if half % 128 == 0 else half
    blocks = half // block

    def like(array):
        return pltpu.VMEM(array.shape, array.dtype)

    def shape(*dims, kind=F32):
        return jax.ShapeDtypeStruct(dims, kind)

    def wide(*dims):
        return pltpu.VMEM(dims, F32)

    def coded():
        return pltpu.VMEM((blocks, rank + SCALE_ROWS, block), BF16)

    dma = pltpu.SemaphoreType.DMA
    v_rows, o_rows = vmas.shape[0], omas.shape[0]
    gathered = pl.pallas_call(
        functools.partial(gather_kernel, fs, tp),
        out_shape=(
            shape(fs, band, columns), shape(rank, columns), shape(rank, columns), shape(fs * o_rows, columns),
            shape(1, 128),
            shape(v_rows, columns), shape(v_rows, columns), shape(fs * v_rows, columns, kind=BF16),
            shape(band, columns), shape(band, columns),
        ),
        in_specs=[HBM] * 12,
        out_specs=(VMEM,) * 10,
        scratch_shapes=[
            like(vfac), like(ofac), like(vin), like(vcot), like(heads), pltpu.VMEM((half, width), BF16),
            like(ocot), pltpu.VMEM((half, columns), BF16), like(vm1), like(vm2), like(vmas),
            wide(blocks, rank, block), wide(blocks, rank, block), wide(blocks, rank, block),
            coded(), coded(), coded(), coded(),
            wide(2 * rank, columns), wide(2 * rank, columns), wide(rank, columns), wide(rank, columns),
            wide(2, fs, band, columns), wide(2, fs, band, columns), wide(1, band, columns),
            wide(fs, band, columns), wide(fs, 1, 128), wide(tp, 1, 128), wide(fs * tp, 1, 128),
            dma((14,)), dma, dma, dma, dma, dma((blocks,)), dma((blocks,)), dma((blocks,)), dma((blocks,)),
            dma, dma, dma((2, fs)), dma((2, fs)), dma((2, fs)), dma((2, fs)), dma((fs,)), dma((fs,)),
            dma((tp,)), dma((tp,)), dma((fs * tp,)), dma((fs * tp,)), dma((2, fs)), dma((2, fs)),
            dma((PIECES, fs)), dma((PIECES, fs)), dma((fs,)), dma((fs,)),
        ],
        compiler_params=pltpu.CompilerParams(
            collective_id=0, has_side_effects=True, vmem_limit_bytes=24 * 1024 * 1024
        ),
    )(*(pltpu.with_memory_space_constraint(a, pltpu.HBM) for a in (
        vin, vcot, vfac, vmas, vm1, vm2, heads, ocot, ofac, omas, om1, om2
    )))
    o_all, o1_all, o2_all, om_all, totals, *values = gathered

    return pl.pallas_call(
        functools.partial(finish_kernel, fs, tp),
        out_shape=(
            shape(v_rows, columns), shape(v_rows, columns), shape(fs * v_rows, columns, kind=BF16),
            shape(band, columns), shape(band, columns),
            shape(o_rows, columns), shape(o_rows, columns), shape(fs * o_rows, columns, kind=BF16),
            shape(band, columns), shape(band, columns),
        ),
        in_specs=[VMEM] * 11,
        out_specs=(HBM,) * 10,
        scratch_shapes=[
            wide(o_rows, columns), wide(o_rows, columns), pltpu.VMEM((fs * o_rows, columns), BF16),
            wide(band, columns), wide(band, columns), dma((9 + fs,)),
        ],
        compiler_params=pltpu.CompilerParams(vmem_limit_bytes=24 * 1024 * 1024),
    )(o_all, o1_all, o2_all, om_all, totals, ofac, *values)


def solution(mesh):
    both = P("fs", "tp")
    in_specs = (both, P("fs", None), P(), both, both, both, both, both, P(), both, both, both)
    out_specs = (
        both, both, P(None, "tp"), both, both, both, both, P(None, "tp"), both, both,
    )
    return jax.shard_map(
        on_device, mesh=mesh, in_specs=in_specs, out_specs=out_specs, check_vma=False
    )
```

time: 50.3 us -> 39.3 us (0.78)
  Pallas kernels: 49.5 us -> 38.4 us
    pallas_call x2, Pallas kernels: 49.5 us -> 38.4 us  [the longest x1 37 us: on_device(): pl.pallas_call(functools.partial(gather_kernel, fs, tp), out_shape=(shape...]
where the time goes in v1:
time: 39.3 us; the launch traced here: 39.1 us
  Pallas kernels  38.4 us (98%)
  between operations  0.67 us (2%)
    pallas_call x1, Pallas kernels, on_device(): pl.pallas_call(functools.partial(gather_kernel, fs, tp), out_shape=(shape...  37 us
    pallas_call x1, Pallas kernels, on_device(): pl.pallas_call(functools.partial(finish_kernel, fs, tp), out_shape=(shape...  1.44 us

profile of v1, /device:TPU:0, one launch (start us, length us, event | category | flops | bytes accessed | tf_op | source)
XLA Modules:
  0.0 39.1 jit_solution(252616915112879890)
XLA Ops:
  0.6 0.0 copy-start
  0.7 37.0 %shard_map.195 = (f32[4,32,256]{2,1,0:T(8,128)S(1)}, f32[128,256]{1,0:T(8,128)S(1)}, f32[128,256]{1,0:T(8,128)S(1)}, f32[1024,256]{1,0:T(8,128)S(1)}, f32[1,128]...) custom-call(bf16[2048,256]{1,0:T(8,128)(2,1)} %vin.1, ...), custom_call_target="tpu_custom_call" | custom-call | tf_op jit(solution)/shard_map/pallas_call | solution.py:462
  37.7 0.0 copy-done
  37.7 1.4 %shard_map.196 = (f32[128,256]{1,0:T(8,128)}, f32[128,256]{1,0:T(8,128)}, bf16[512,256]{1,0:T(8,128)(2,1)}, f32[32,256]{1,0:T(8,128)}, f32[32,256]{1,0:T(8,128)}...) custom-call(f32[4,32,256]{2,1,0:T(8,128)S(1)} %get-tuple-element.20., ...), custom_call_target="tpu_custom_call" | custom-call | tf_op jit(solution)/shard_map/pallas_call | solution.py:493
Async XLA Ops:
  0.6 37.0 %copy-start = (bf16[1024,128]{1,0:T(8,128)(2,1)S(1)}, bf16[1024,128]{1,0:T(8,128)(2,1)}, u32[]{:S(2)}) copy-start(bf16[1024,128]{1,0:T(8,128)(2,1)} %ofac.3) | copy-start | bytes 786436

commit v2 on v1

v2 whole, which is shorter than its diff:
```python
import functools

import jax
import jax.numpy as jnp
from jax import lax
from jax.experimental import pallas as pl
from jax.experimental.pallas import tpu as pltpu
from jax.sharding import PartitionSpec as P

MESH = pl.DeviceIdType.MESH
ANY = pl.BlockSpec(memory_space=pl.ANY)
HBM = pl.BlockSpec(memory_space=pltpu.HBM)
VMEM = pl.BlockSpec(memory_space=pltpu.VMEM)
BF16 = jnp.bfloat16
F32 = jnp.float32
PRE = 3
SUF = 4
LEVELS = 252.0
POWER = 15
PEAK = 320.0


def split(wide, axis):
    high = wide.astype(BF16)
    low = (wide - high.astype(F32)).astype(BF16)
    return jnp.concatenate([high, low], axis=axis)


def encode(x, top):
    u = x * (PEAK / top)
    u3 = u * u * u
    u5 = u3 * u * u
    return (u5 * u5 * u5).astype(BF16)


def decode(coded, top):
    y = coded.astype(F32)
    size = jnp.abs(y)
    root = jnp.exp(jnp.log(jnp.maximum(size, 1e-37)) * (1.0 / POWER))
    root = jnp.where(size < 2e-37, 0.0, root) * (top * (1.0 / PEAK))
    return jnp.where(y < 0.0, -root, root)


def encode_even(x, top):
    size = jnp.exp2(jnp.abs(x) * (LEVELS / top) - LEVELS / 2)
    return jnp.where(x < 0.0, -size, size).astype(BF16)


def decode_even(coded, top):
    y = coded.astype(F32)
    size = (jnp.log2(jnp.maximum(jnp.abs(y), 1e-38)) + LEVELS / 2) * (top * (1.0 / LEVELS))
    return jnp.where(y < 0.0, -size, size)


def top_of(x):
    return jnp.max(jnp.abs(x), axis=0, keepdims=True) * 1.02 + 1e-30


def gather_kernel(
    fs, tp,
    vin, vcot, vfac, vmas, vm1, vm2, heads, ocot, ofac, omas, om1, om2,
    o_all, o1_all, o2_all, om_all, totals, v_step, v_new, v_copy, v_first, v_second,
    vfac_v, ofac_v, vin_v, vcot_v, heads_v, heads_in, ocot_v, ocot_in, v1_v, v2_v, vm_v, om_v,
    own_v, left_v, right_v, pre_in, pre_out, suf_in, suf_out, tops, acc_own, acc_pair, pair_out, pair_in,
    swap, swap_top, proj_v, dir_all, sums, mas, mas_top,
    load_sem, heads_send, heads_recv, ocot_send, ocot_recv, pre_send, pre_recv, suf_send, suf_recv, tops_send, tops_recv,
    pair_send, pair_recv, swap_send, swap_recv, mark_send, mark_recv, dir_send, dir_recv, sum_send, sum_recv,
    mom_send, mom_recv, mas_send, mas_recv, mast_send, mast_recv, copy_send, copy_recv,
):
    f = lax.axis_index("fs")
    t = lax.axis_index("tp")
    chip = t // 2
    core = t % 2
    chips = tp // 2
    last = chips - 1
    rank = vfac.shape[1]
    band = rank // fs
    tokens, width = heads.shape
    columns = vin.shape[1]
    half = tokens // 2
    blocks, part, block = own_v.shape
    both = rank // part
    o_rows = omas.shape[0]
    mine_at = pl.multiple_of(core * half, half)
    pair_at = pl.multiple_of((1 - core) * half, half)
    scope = jax.named_scope

    fs_peers = [3 - f, f + 1 - 2 * (f % 2), lax.rem(f + 2, fs)] if fs == 4 else [lax.rem(f + j, fs) for j in range(1, fs)]

    def tp_peer(j):
        return lax.rem(t + j, tp)

    def own_rows(ref):
        rows = ref.shape[0] // fs
        return ref.at[pl.ds(pl.multiple_of(f * rows, rows), rows)]

    jobs = [
        (heads.at[pl.ds(pair_at, half)], heads_v.at[pl.ds(pair_at, half)]),
        (ofac, ofac_v),
        (heads.at[pl.ds(mine_at, half)], heads_v.at[pl.ds(mine_at, half)]),
        (om1, own_rows(o1_all)), (om2, own_rows(o2_all)),
        (vfac, vfac_v), (vcot, vcot_v), (vin, vin_v), (omas, om_v),
        (ocot.at[pl.ds(pair_at, half)], ocot_v.at[pl.ds(pair_at, half)]),
        (ocot.at[pl.ds(mine_at, half)], ocot_v.at[pl.ds(mine_at, half)]),
        (vmas, vm_v), (vm1, v1_v), (vm2, v2_v),
    ]
    loads = [pltpu.make_async_copy(a, b, load_sem.at[i]) for i, (a, b) in enumerate(jobs)]
    for load in loads:
        load.start()

    partner = {"tp": chip * 2 + (1 - core)}
    right = {"tp": lax.rem(t + 2, tp)}
    left = {"tp": lax.rem(t + tp - 2, tp)}
    barrier = pltpu.get_barrier_semaphore()

    def greet(where):
        pl.semaphore_signal(barrier, inc=1, device_id=where, device_id_type=MESH)

    greet(partner)
    for d in fs_peers:
        greet({"fs": d})

    @pl.when(chip > 0)
    def _():
        greet(left)

    @pl.when(chip < last)
    def _():
        greet(right)

    with scope("barrier"):
        pl.semaphore_wait(barrier, fs + (chip + last) // chips + (last - chip + last) // chips)

    def remote(src, dst, send_sem, recv_sem, where):
        return pltpu.make_async_remote_copy(
            src_ref=src, dst_ref=dst, send_sem=send_sem, recv_sem=recv_sem,
            device_id=where, device_id_type=MESH,
        )

    def send(src, dst, send_sem, recv_sem, where):
        remote(src, dst, send_sem, recv_sem, where).start()

    def landed(dst, sem):
        remote(dst, dst, sem, sem, partner).wait_recv()

    def left_here(src, sem):
        remote(src, src, sem, sem, partner).wait_send()

    with scope("heads_load"):
        loads[0].wait()
    send(heads_v.at[pl.ds(pair_at, half)], heads_in, heads_send, heads_recv, partner)
    for i, whole in ((3, o1_all), (4, o2_all)):
        loads[i].wait()
        here = own_rows(whole)
        for d in fs_peers:
            send(here, here, mom_send, mom_recv, {"fs": d})


    def masters_send(start, rows):
        here = mas.at[f, pl.ds(start, rows)]
        for d in fs_peers:
            send(here, here, mas_send, mas_recv, {"fs": d})

    def masters_first():
        loads[8].wait()
        top = top_of(om_v[...])
        mas_top[f] = top
        mas[f] = encode_even(om_v[...], top)
        for d in fs_peers:
            send(mas_top.at[f], mas_top.at[f], mast_send, mast_recv, {"fs": d})
        masters_send(0, o_rows)

    def masters_end():
        landed(mas_top.at[pl.ds(0, fs - 1)], mast_recv)
        landed(mas.at[pl.ds(0, fs - 1)], mas_recv)
        for g in range(fs):
            om_all[pl.ds(g * o_rows, o_rows), :] = decode_even(mas[g], mas_top[g])

    with scope("factor_load"):
        loads[1].wait()
        loads[2].wait()

    def factor_of(s):
        rows = ofac_v[pl.ds(pl.multiple_of(s * width, width), width), :]
        return rows.astype(F32).T.astype(BF16)

    def against(left, right):
        return lax.dot_general(left, right, (((1,), (1,)), ((), ())), preferred_element_type=F32)

    def to_right(k):
        return remote(pre_out.at[k], pre_in.at[k], pre_send, pre_recv.at[k], right)

    def to_left(k):
        return remote(suf_out.at[k], suf_in.at[k], suf_send, suf_recv.at[k], left)

    def top_right(top):
        tops[3] = top
        send(tops.at[3], tops.at[1], tops_send.at[0], tops_recv.at[0], right)

    def top_left(top):
        tops[4] = top
        send(tops.at[4], tops.at[2], tops_send.at[1], tops_recv.at[1], left)

    factor_mine = factor_of(t)
    factor_pair = factor_of(chip * 2 + (1 - core))
    with scope("heads_in"):
        landed(heads_in, heads_recv)
    with scope("own"):
        top = jnp.zeros((rank, block), F32)
        for k in range(half // block):
            here = heads_v[pl.ds(pl.multiple_of(mine_at + k * block, block), block), :]
            own = against(factor_mine, here) + against(factor_pair, heads_in[pl.ds(k * block, block), :])
            top = jnp.maximum(top, jnp.abs(own))
            own_v[pl.ds(k * both, both)] = own.reshape(both, part, block)
        top = top_of(top)
        tops[0] = top

    @pl.when(chip == 0)
    def _():
        top_right(top)
        left_v[...] = jnp.zeros_like(left_v)

        def first(k, _):
            pre_out[k] = encode(own_v[k], tops[3])
            to_right(k).start()
            return 0

        lax.fori_loop(0, blocks, first, 0)

    @pl.when(chip == last)
    def _():
        top_left(top)
        right_v[...] = jnp.zeros_like(right_v)

        def first(k, _):
            suf_out[k] = encode(own_v[k], tops[4])
            to_left(k).start()
            return 0

        lax.fori_loop(0, blocks, first, 0)

    with scope("ocot_load"):
        loads[9].wait()
        loads[10].wait()
    send(ocot_v.at[pl.ds(pair_at, half)], ocot_in, ocot_send, ocot_recv, partner)

    def exchange(k, mine):
        top = top_of(mine)
        swap_top[k, f] = top
        swap[k, f] = encode(mine, top)
        for d in fs_peers:
            send(swap_top.at[k, f], swap_top.at[k, f], mark_send.at[k], mark_recv.at[k], {"fs": d})
            send(swap.at[k, f], swap.at[k, f], swap_send.at[k], swap_recv.at[k], {"fs": d})

    def exchanged(k):
        landed(swap_top.at[k, pl.ds(0, fs - 1)], mark_recv.at[k])
        landed(swap.at[k, pl.ds(0, fs - 1)], swap_recv.at[k])
        whole = decode(swap[k, 0], swap_top[k, 0])
        for g in range(1, fs):
            whole = whole + decode(swap[k, g], swap_top[k, g])
        return whole

    def sum_out(k, whole):
        sums[k, t] = jnp.sum(whole * whole, axis=0, keepdims=True)
        for j in range(1, tp):
            send(sums.at[k, t], sums.at[k, t], sum_send.at[k], sum_recv.at[k], {"tp": tp_peer(j)})

    def sum_in(k):
        landed(sums.at[k, pl.ds(0, tp - 1)], sum_recv.at[k])
        return jnp.sum(sums[k], axis=0)

    with scope("value_load"):
        for i in (5, 6, 7):
            loads[i].wait()
    with scope("value_compute"):
        total = jnp.zeros((2 * rank, columns), F32)
        stride = 256 if tokens % 256 == 0 else tokens
        for i in range(tokens // stride):
            rows = pl.ds(i * stride, stride)
            image = jnp.dot(vcot_v[rows, :], vfac_v[...], preferred_element_type=F32)
            total = total + lax.dot_general(
                split(image, 1), vin_v[rows, :], (((0,), (0,)), ((), ())), preferred_element_type=F32
            )
        exchange(0, total[:rank] + total[rank:])
    with scope("masters_first"):
        masters_first()
    with scope("ocot_in"):
        landed(ocot_in, ocot_recv)
    acc_own[...] = jnp.zeros_like(acc_own)
    acc_pair[...] = jnp.zeros_like(acc_pair)

    def step(i, _):
        k = i - PRE * chip

        @pl.when((chip > 0) & (k >= 0) & (k < blocks))
        def _():
            @pl.when(k == 0)
            def _():
                landed(tops.at[1], tops_recv.at[0])

                @pl.when(chip < last)
                def _():
                    top_right(tops[0] + tops[1])

            with scope("pre_wait"):
                landed(pre_in.at[k], pre_recv.at[k])
            left_v[k] = decode(pre_in[k], tops[1])

            @pl.when(chip < last)
            def _():
                pre_out[k] = encode(left_v[k] + own_v[k], tops[3])
                to_right(k).start()

        m = i - SUF * (last - chip)

        @pl.when((chip < last) & (m >= 0) & (m < blocks))
        def _():
            @pl.when(m == 0)
            def _():
                landed(tops.at[2], tops_recv.at[1])

                @pl.when(chip > 0)
                def _():
                    top_left(tops[0] + tops[2])

            with scope("suf_wait"):
                landed(suf_in.at[m], suf_recv.at[m])
            right_v[m] = decode(suf_in[m], tops[2])

            @pl.when(chip > 0)
            def _():
                suf_out[m] = encode(right_v[m] + own_v[m], tops[4])
                to_left(m).start()

        n = i - jnp.maximum(PRE * chip, SUF * (last - chip))

        @pl.when((n >= 0) & (n < blocks) & (lax.rem(n + both, both) == both - 1))
        def _():
            with scope("acc"):
                group = lax.div(n, both)
                these = pl.ds(group * both, both)
                two = split((left_v[these] + own_v[these] + right_v[these]).reshape(rank, block), 0)
                here = pl.ds(pl.multiple_of(mine_at + group * block, block), block)
                there = pl.ds(pl.multiple_of(group * block, block), block)
                acc_own[...] += jnp.dot(two, ocot_v[here, :], preferred_element_type=F32)
                acc_pair[...] += jnp.dot(two, ocot_in[there, :], preferred_element_type=F32)

        return 0

    def value_sums():
        whole = exchanged(0)
        proj_v[...] = whole
        sum_out(0, whole)

    def value_direction():
        total = jnp.sum(sum_in(0), axis=1, keepdims=True)
        scale = lax.rsqrt(total / (rank * columns * tp) + 1e-06)
        for i in (12, 13):
            loads[i].wait()
        scaled = scale * own_rows(proj_v)[...]
        first_new = 0.9 * v1_v[...] + 0.1 * scaled
        second_new = 0.95 * v2_v[...] + 0.05 * scaled * scaled
        v_first[...] = first_new
        v_second[...] = second_new
        dir_all[f] = first_new / (jnp.sqrt(second_new) + 1e-08)
        for d in fs_peers:
            send(dir_all.at[f], dir_all.at[f], dir_send, dir_recv, {"fs": d})

    def value_finish():
        landed(dir_all.at[pl.ds(0, fs - 1)], dir_recv)
        direction = split(dir_all[...].reshape(rank, columns), 0)
        count = v_step.shape[0]
        left = vfac_v[pl.ds(pl.multiple_of(f * count, count), count), :]
        move = jnp.dot(jnp.concatenate([left, left], axis=1), direction, preferred_element_type=F32)
        loads[11].wait()
        fresh = vm_v[...] - 0.002 * move
        v_step[...] = move
        v_new[...] = fresh
        here = own_rows(v_copy)
        here[...] = fresh.astype(BF16)
        for d in fs_peers:
            send(here, here, copy_send, copy_recv, {"fs": d})

    steps = blocks + max(PRE, SUF) * last
    done = 0
    for at, event in ((13, value_sums), (steps - 2, value_direction)):
        at = min(at, steps)
        lax.fori_loop(done, at, step, 0)
        done = at
        with scope(f"event{at}"):
            event()
    lax.fori_loop(done, steps, step, 0)

    pair_out[...] = acc_pair[:rank, :] + acc_pair[rank:, :]
    send(pair_out, pair_in, pair_send, pair_recv, partner)
    mine = acc_own[:rank, :] + acc_own[rank:, :]
    with scope("pair_wait"):
        landed(pair_in, pair_recv)
    with scope("exchange"):
        exchange(1, mine + pair_in[...])
    with scope("value_finish"):
        value_finish()
    with scope("exchanged"):
        whole = exchanged(1)
        o_all[...] = whole
        sum_out(1, whole)
    with scope("mom_wait"):
        moments = om_all.at[pl.ds(0, 2 * (fs - 1) * band)]
        landed(moments, mom_recv)
        left_here(moments, mom_send)
    with scope("masters_wait"):
        masters_end()
    with scope("copy_wait"):
        copies = v_copy.at[pl.ds(0, (fs - 1) * v_step.shape[0])]
        landed(copies, copy_recv)
        left_here(copies, copy_send)
    with scope("drain"):
        left_here(heads_in, heads_send)
        left_here(mas.at[pl.ds(0, fs - 1)], mas_send)
        left_here(mas_top.at[pl.ds(0, fs - 1)], mast_send)
        left_here(ocot_in, ocot_send)
        left_here(pair_out, pair_send)

        @pl.when(chip < last)
        def _():
            left_here(pre_out, pre_send)
            left_here(tops.at[3], tops_send.at[0])

        @pl.when(chip > 0)
        def _():
            left_here(suf_out, suf_send)
            left_here(tops.at[4], tops_send.at[1])

        for k in range(2):
            left_here(swap.at[k, pl.ds(0, fs - 1)], swap_send.at[k])
            left_here(swap_top.at[k, pl.ds(0, fs - 1)], mark_send.at[k])
        left_here(dir_all.at[pl.ds(0, fs - 1)], dir_send)
        left_here(sums.at[0, pl.ds(0, tp - 1)], sum_send.at[0])
    with scope("sums_wait"):
        totals[...] = sum_in(1)
        left_here(sums.at[1, pl.ds(0, tp - 1)], sum_send.at[1])


def finish_kernel(
    fs, tp,
    o_all, o1_all, o2_all, om_all, totals, ofac, omas, v_step, v_new, v_copy, v_first, v_second,
    v_step_out, v_new_out, v_copy_out, v_first_out, v_second_out,
    o_step_out, o_new_out, o_copy_out, o_first_out, o_second_out,
    step_v, new_v, copy_v, first_v, second_v, out_sem,
):
    f = lax.axis_index("fs")
    puts = []

    def put(src, dst):
        copy = pltpu.make_async_copy(src, dst, out_sem.at[len(puts)])
        copy.start()
        puts.append(copy)

    for src, dst in (
        (v_step, v_step_out), (v_new, v_new_out), (v_copy, v_copy_out), (v_first, v_first_out), (v_second, v_second_out),
    ):
        put(src, dst)
    rank, columns = o1_all.shape
    band = rank // fs
    total = jnp.sum(totals[...], axis=1, keepdims=True)
    scale = lax.rsqrt(total / (rank * columns * tp) + 1e-06)

    def moments(proj, rows):
        scaled = scale * proj
        first_new = 0.9 * o1_all[rows, :] + 0.1 * scaled
        second_new = 0.95 * o2_all[rows, :] + 0.05 * scaled * scaled
        return first_new, second_new

    own_band = pl.ds(pl.multiple_of(f * band, band), band)
    first_v[...], second_v[...] = moments(o_all[own_band, :], pl.ds(pl.multiple_of(f * band, band), band))
    put(first_v, o_first_out)
    put(second_v, o_second_out)
    first_new, second_new = moments(o_all[...], pl.ds(0, rank))
    direction = split(first_new / (jnp.sqrt(second_new) + 1e-08), 0)

    def step_of(rows):
        left = ofac[rows, :]
        return jnp.dot(jnp.concatenate([left, left], axis=1), direction, preferred_element_type=F32)

    count = step_v.shape[0]
    own = pl.ds(pl.multiple_of(f * count, count), count)
    move = step_of(own)
    step_v[...] = move
    put(step_v, o_step_out)
    new_v[...] = omas[...] - 0.002 * move
    put(new_v, o_new_out)
    for i in range(fs):
        rows = pl.ds(i * count, count)
        copy_v[rows, :] = (om_all[rows, :] - 0.002 * step_of(rows)).astype(BF16)
        put(copy_v.at[rows], o_copy_out.at[rows])
    for copy in puts:
        copy.wait()


def on_device(vin, vcot, vfac, vmas, vm1, vm2, heads, ocot, ofac, omas, om1, om2):
    fs = lax.axis_size("fs")
    tp = lax.axis_size("tp")
    rank = vfac.shape[1]
    band = rank // fs
    columns = vin.shape[1]
    tokens, width = heads.shape
    half = tokens // 2
    block = 128 if half % 128 == 0 else half
    part = rank
    blocks = half // block * (rank // part)

    def like(array):
        return pltpu.VMEM(array.shape, array.dtype)

    def shape(*dims, kind=F32):
        return jax.ShapeDtypeStruct(dims, kind)

    def wide(*dims):
        return pltpu.VMEM(dims, F32)

    def coded():
        return pltpu.VMEM((blocks, part, block), BF16)

    dma = pltpu.SemaphoreType.DMA
    v_rows, o_rows = vmas.shape[0], omas.shape[0]
    gathered = pl.pallas_call(
        functools.partial(gather_kernel, fs, tp),
        out_shape=(
            shape(rank, columns), shape(rank, columns), shape(rank, columns), shape(fs * o_rows, columns),
            shape(1, columns),
            shape(v_rows, columns), shape(v_rows, columns), shape(fs * v_rows, columns, kind=BF16),
            shape(band, columns), shape(band, columns),
        ),
        in_specs=[HBM] * 12,
        out_specs=(VMEM,) * 10,
        scratch_shapes=[
            like(vfac), like(ofac), like(vin), like(vcot), like(heads), pltpu.VMEM((half, width), BF16),
            like(ocot), pltpu.VMEM((half, columns), BF16), like(vm1), like(vm2), like(vmas), like(omas),
            wide(blocks, part, block), wide(blocks, part, block), wide(blocks, part, block),
            coded(), coded(), coded(), coded(), wide(5, 1, block),
            wide(2 * rank, columns), wide(2 * rank, columns), wide(rank, columns), wide(rank, columns),
            pltpu.VMEM((2, fs, rank, columns), BF16), wide(2, fs, 1, columns), wide(rank, columns),
            wide(fs, band, columns), wide(2, tp, 1, columns),
            pltpu.VMEM((fs, o_rows, columns), BF16), wide(fs, 1, columns),
            dma((14,)), dma, dma, dma, dma, dma, dma((blocks,)), dma, dma((blocks,)), dma((2,)), dma((2,)),
            dma, dma, dma((2,)), dma((2,)), dma((2,)), dma((2,)), dma, dma, dma((2,)), dma((2,)),
            dma, dma, dma, dma, dma, dma, dma, dma,
        ],
        compiler_params=pltpu.CompilerParams(
            collective_id=0, has_side_effects=True, vmem_limit_bytes=24 * 1024 * 1024
        ),
    )(*(pltpu.with_memory_space_constraint(a, pltpu.HBM) for a in (
        vin, vcot, vfac, vmas, vm1, vm2, heads, ocot, ofac, omas, om1, om2
    )))
    o_all, o1_all, o2_all, om_all, totals, *values = gathered

    return pl.pallas_call(
        functools.partial(finish_kernel, fs, tp),
        out_shape=(
            shape(v_rows, columns), shape(v_rows, columns), shape(fs * v_rows, columns, kind=BF16),
            shape(band, columns), shape(band, columns),
            shape(o_rows, columns), shape(o_rows, columns), shape(fs * o_rows, columns, kind=BF16),
            shape(band, columns), shape(band, columns),
        ),
        in_specs=[VMEM] * 12,
        out_specs=(HBM,) * 10,
        scratch_shapes=[
            wide(o_rows, columns), wide(o_rows, columns), pltpu.VMEM((fs * o_rows, columns), BF16),
            wide(band, columns), wide(band, columns), dma((9 + fs,)),
        ],
        compiler_params=pltpu.CompilerParams(vmem_limit_bytes=24 * 1024 * 1024),
    )(o_all, o1_all, o2_all, om_all, totals, ofac, omas, *values)


def solution(mesh):
    both = P("fs", "tp")
    in_specs = (both, P("fs", None), P(), both, both, both, both, both, P(), both, both, both)
    out_specs = (
        both, both, P(None, "tp"), both, both, both, both, P(None, "tp"), both, both,
    )
    return jax.shard_map(
        on_device, mesh=mesh, in_specs=in_specs, out_specs=out_specs, check_vma=False
    )
```

time: 39.3 us -> 33.3 us (0.85)
  Pallas kernels: 38.4 us -> 32.5 us
    pallas_call x1, Pallas kernels: 37 us -> 31 us  [on_device(): pl.pallas_call(functools.partial(gather_kernel, fs, tp), out_shape=(shape...]
where the time goes in v2:
time: 33.3 us; the launch traced here: 33.2 us
  Pallas kernels  32.5 us (98%)
  between operations  0.69 us (2%)
    pallas_call x1, Pallas kernels, on_device(): pl.pallas_call(functools.partial(gather_kernel, fs, tp), out_shape=(shape...  31 us
    pallas_call x1, Pallas kernels, on_device(): pl.pallas_call(functools.partial(finish_kernel, fs, tp), out_shape=(shape...  1.45 us

profile of v2, /device:TPU:0, one launch (start us, length us, event | category | flops | bytes accessed | tf_op | source)
XLA Modules:
  0.0 33.2 jit_solution(1624105773181515967)
XLA Ops:
  0.6 0.0 copy-start.1
  0.7 0.0 copy-start
  0.7 31.0 %shard_map.195 = (f32[128,256]{1,0:T(8,128)S(1)}, f32[128,256]{1,0:T(8,128)S(1)}, f32[128,256]{1,0:T(8,128)S(1)}, f32[1024,256]{1,0:T(8,128)S(1)}, f32[1,256]{1,...) custom-call(bf16[2048,256]{1,0:T(8,128)(2,1)} %vin.1, ...), custom_call_target="tpu_custom_call" | custom-call | tf_op jit(solution)/shard_map/pallas_call | solution.py:526
  31.7 0.0 copy-done.1
  31.7 0.0 copy-done
  31.7 1.4 %shard_map.196 = (f32[128,256]{1,0:T(8,128)}, f32[128,256]{1,0:T(8,128)}, bf16[512,256]{1,0:T(8,128)(2,1)}, f32[32,256]{1,0:T(8,128)}, f32[32,256]{1,0:T(8,128)}...) custom-call(f32[128,256]{1,0:T(8,128)S(1)} %get-tuple-element.20.o_a, ...), custom_call_target="tpu_custom_call" | custom-call | tf_op jit(solution)/shard_map/pallas_call | solution.py:557
Async XLA Ops:
  0.6 31.0 %copy-start.1 = (f32[256,256]{1,0:T(8,128)S(1)}, f32[256,256]{1,0:T(8,128)}, u32[]{:S(2)}) copy-start(f32[256,256]{1,0:T(8,128)} %omas.3) | copy-start | bytes 786436
  0.7 31.0 %copy-start = (bf16[1024,128]{1,0:T(8,128)(2,1)S(1)}, bf16[1024,128]{1,0:T(8,128)(2,1)}, u32[]{:S(2)}) copy-start(bf16[1024,128]{1,0:T(8,128)(2,1)} %ofac.3) | copy-start | bytes 786436

commit v3 on v2

v3 whole, which is shorter than its diff:
```python
import functools

import jax
import jax.numpy as jnp
from jax import lax
from jax.experimental import pallas as pl
from jax.experimental.pallas import tpu as pltpu
from jax.sharding import PartitionSpec as P

MESH = pl.DeviceIdType.MESH
ANY = pl.BlockSpec(memory_space=pl.ANY)
HBM = pl.BlockSpec(memory_space=pltpu.HBM)
VMEM = pl.BlockSpec(memory_space=pltpu.VMEM)
BF16 = jnp.bfloat16
F32 = jnp.float32
PRE = 5
SUF = 7
LEVELS = 252.0
POWER = 7
PEAK = 240000.0
HEADS_BOUND = 6.0
HEADS_PIECES = 4


def split(wide, axis):
    high = wide.astype(BF16)
    low = (wide - high.astype(F32)).astype(BF16)
    return jnp.concatenate([high, low], axis=axis)


def encode(x, top):
    u = x * (PEAK / top)
    u2 = u * u
    return (u2 * u2 * u2 * u).astype(BF16)


def decode(coded, top):
    y = coded.astype(F32)
    size = jnp.abs(y)
    root = jnp.exp(jnp.log(jnp.maximum(size, 1e-37)) * (1.0 / POWER))
    root = jnp.where(size < 2e-37, 0.0, root) * (top * (1.0 / PEAK))
    return jnp.where(y < 0.0, -root, root)


def encode_even(x, top):
    size = jnp.exp2(jnp.abs(x) * (LEVELS / top) - LEVELS / 2)
    return jnp.where(x < 0.0, -size, size).astype(BF16)


def decode_even(coded, top):
    y = coded.astype(F32)
    size = (jnp.log2(jnp.maximum(jnp.abs(y), 1e-38)) + LEVELS / 2) * (top * (1.0 / LEVELS))
    return jnp.where(y < 0.0, -size, size)


def top_of(x):
    return jnp.max(jnp.abs(x), axis=0, keepdims=True) * 1.02 + 1e-30


def gather_kernel(
    fs, tp,
    vin, vcot, vfac, vmas, vm1, vm2, heads, ocot, ofac, omas, om1, om2,
    o_all, o1_all, o2_all, om_all, totals, v_step, v_new, v_copy, v_first, v_second,
    vfac_v, ofac_v, vin_v, vcot_v, image_v, heads_v, heads_in, ocot_v, ocot_in, v1_v, v2_v, vm_v, om_v, o1_v, o2_v,
    own_v, left_v, right_v, pre_in, pre_out, suf_in, suf_out, bound, acc_own, acc_pair,
    pair_out, pair_top, swap, swap_top, value_swap, value_top, proj_v, mom, mom_top, value_mom, value_momt, sums, value_sums, mas, mas_top,
    pair_mas, pair_mast, back_first, back_second, back_step, back_new, back_copy, stage,
    load_sem, heads_send, heads_recv, ocot_send, ocot_recv, gift_send, gift_recv, pre_send, pre_recv, suf_send, suf_recv,
    swap_send, swap_recv, mark_send, mark_recv, sum_send, sum_recv, seen,
    mom_send, mom_recv, momt_send, momt_recv, mas_send, mas_recv, mast_send, mast_recv, give_send, give_recv, back_send, back_recv, copy_send, copy_recv,
):
    f = lax.axis_index("fs")
    t = lax.axis_index("tp")
    chip = t // 2
    core = t % 2
    chips = tp // 2
    last = chips - 1
    rank = vfac.shape[1]
    band = rank // fs
    tokens, width = heads.shape
    columns = vin.shape[1]
    blocks, _, block = own_v.shape
    o_rows = omas.shape[0]
    v_rows = vmas.shape[0]
    piece = tokens // HEADS_PIECES
    scope = jax.named_scope
    hub = core == 1
    aide = core == 0
    at_last = (last - chip + last) // chips
    at_first = (chip + last) // chips

    fs_peers = [3 - f, f + 1 - 2 * (f % 2), lax.rem(f + 2, fs)] if fs == 4 else [lax.rem(f + j, fs) for j in range(1, fs)]
    partner = {"tp": chip * 2 + (1 - core)}
    right = {"tp": lax.rem(t + 2, tp)}
    left = {"tp": lax.rem(t + tp - 2, tp)}

    def own_rows(ref):
        rows = ref.shape[0] // fs
        return ref.at[pl.ds(pl.multiple_of(f * rows, rows), rows)]

    pieces = [pl.ds(i * piece, piece) for i in range(HEADS_PIECES)]
    count = HEADS_PIECES

    def loading(i, src, dst):
        return pltpu.make_async_copy(src, dst, load_sem.at[i])

    heads_load = [loading(i, heads.at[rows], heads_v.at[rows]) for i, rows in enumerate(pieces)]
    om1_load = loading(count, om1, o1_v)
    om2_load = loading(count + 1, om2, o2_v)
    omas_load = loading(count + 2, omas, om_v)
    ocot_load = loading(count + 3, ocot, ocot_v)
    ofac_load = loading(count + 4, ofac, ofac_v)
    vfac_load = loading(count + 4, vfac, vfac_v)
    vcot_load = loading(count + 5, vcot, vcot_v)
    vin_load = loading(count + 6, vin, vin_v.at[0])
    vm1_load = loading(count + 7, vm1, v1_v.at[0])
    vm2_load = loading(count + 8, vm2, v2_v.at[0])
    vmas_load = loading(count + 9, vmas, vm_v.at[0])

    heads_load[0].start()

    @pl.when(hub)
    def _():
        ofac_load.start()

    for load in (*heads_load[1:], om1_load, om2_load):
        load.start()

    @pl.when(hub)
    def _():
        for load in (omas_load, ocot_load):
            load.start()

    @pl.when(aide)
    def _():
        for load in (ocot_load, vfac_load, vcot_load, vin_load, omas_load, vm1_load, vm2_load, vmas_load):
            load.start()

    barrier = pltpu.get_barrier_semaphore()

    def signal(sem, where):
        pl.semaphore_signal(sem, inc=1, device_id=where, device_id_type=MESH)

    signal(barrier, partner)
    for d in fs_peers:
        signal(barrier, {"fs": d})

    @pl.when(chip > 0)
    def _():
        signal(barrier, left)

    @pl.when(chip < last)
    def _():
        signal(barrier, right)

    with scope("barrier"):
        pl.semaphore_wait(barrier, fs + at_first + at_last)

    def pass_right(where):
        @pl.when(where & (chip > 0))
        def _():
            pl.semaphore_wait(seen.at[0], 1)

        @pl.when(where & (chip < last))
        def _():
            signal(seen.at[0], right)

    def pass_left(where):
        @pl.when(where & (chip < last))
        def _():
            pl.semaphore_wait(seen.at[1], 1)

        @pl.when(where & (chip > 0))
        def _():
            signal(seen.at[1], left)

    near = chips // 2

    def remote(src, dst, send_sem, recv_sem, where):
        return pltpu.make_async_remote_copy(
            src_ref=src, dst_ref=dst, send_sem=send_sem, recv_sem=recv_sem,
            device_id=where, device_id_type=MESH,
        )

    def send(src, dst, send_sem, recv_sem, where):
        remote(src, dst, send_sem, recv_sem, where).start()

    def landed(dst, sem):
        remote(dst, dst, sem, sem, partner).wait_recv()

    def left_here(src, sem):
        remote(src, src, sem, sem, partner).wait_send()

    def factor_of(s):
        rows = ofac_v[pl.ds(pl.multiple_of(s * width, width), width), :]
        return rows.astype(F32).T.astype(BF16)

    def against(one, two):
        return lax.dot_general(one, two, (((1,), (1,)), ((), ())), preferred_element_type=F32)

    def to_right(k):
        return remote(pre_out.at[k], pre_in.at[k], pre_send, pre_recv.at[k], right)

    def to_left(k):
        return remote(suf_out.at[k], suf_in.at[k], suf_send, suf_recv.at[k], left)

    def send_moments():
        for i, (load, local) in enumerate(((om1_load, o1_v), (om2_load, o2_v))):
            load.wait()
            top = top_of(local[...])
            mom_top[f, i] = top
            mom[f, i] = encode_even(local[...], top)
        for d in fs_peers:
            send(mom_top.at[f], mom_top.at[f], momt_send.at[0], momt_recv.at[0], {"fs": d})
            send(mom.at[f], mom.at[f], mom_send.at[0], mom_recv.at[0], {"fs": d})

    def masters_encode():
        omas_load.wait()
        top = top_of(om_v[...])
        mas_top[f] = top
        mas[f] = encode_even(om_v[...], top)

    def masters_end():
        landed(mas_top.at[pl.ds(0, fs - 1)], mast_recv)
        landed(mas.at[pl.ds(0, fs - 1)], mas_recv)
        for g in range(fs):
            om_all[pl.ds(g * o_rows, o_rows), :] = decode_even(mas[g], mas_top[g])

    late = at_first * at_last * SUF

    def step(i, _):
        k = i - PRE * chip

        @pl.when((chip > 0) & (k >= 0) & (k < blocks))
        def _():
            with scope("pre_wait"):
                landed(pre_in.at[k], pre_recv.at[k])
            left_v[k] = decode(pre_in[k], bound[...])

            @pl.when(chip < last)
            def _():
                pre_out[k] = encode(left_v[k] + own_v[k], bound[...])
                to_right(k).start()

        m = i - SUF * (last - chip)

        @pl.when((chip < last) & (m >= 0) & (m < blocks))
        def _():
            with scope("suf_wait"):
                landed(suf_in.at[m], suf_recv.at[m])
            right_v[m] = decode(suf_in[m], bound[...])

            @pl.when(chip > 0)
            def _():
                suf_out[m] = encode(right_v[m] + own_v[m], bound[...])
                to_left(m).start()

        n = i - late - jnp.maximum(PRE * chip, SUF * (last - chip))

        @pl.when((n >= 0) & (n < blocks) & (lax.rem(n + 2, 2) == 1))
        def _():
            with scope("acc"):
                image = jnp.concatenate([left_v[j] + own_v[j] + right_v[j] for j in (n - 1, n)], axis=1)
                two = split(image, 0)
                here = pl.ds(pl.multiple_of((n - 1) * block, block), 2 * block)
                acc_own[...] += jnp.dot(two, ocot_v[here, :], preferred_element_type=F32)
                acc_pair[...] += jnp.dot(two, ocot_in[here, :], preferred_element_type=F32)

        return 0

    steps = blocks + SUF * last

    @pl.when(hub)
    def _():
        for i, (src, dst) in enumerate(((vin, vin_v), (vm1, v1_v), (vm2, v2_v), (vmas, vm_v))):
            send(src, dst.at[1], gift_send.at[i], gift_recv.at[i], partner)
        send_moments()
        with scope("factor"):
            ofac_load.wait()
            reach = jnp.sum(jnp.abs(ofac_v[...].astype(F32)), axis=0, keepdims=True)
            top = jnp.max(reach, axis=1, keepdims=True) * (1.02 * HEADS_BOUND) + 1e-30
            bound[...] = jnp.broadcast_to(top, bound.shape)
            factor = jnp.concatenate([factor_of(t - 1), factor_of(t)], axis=1)
        group = blocks // HEADS_PIECES
        for i, rows in enumerate(pieces):
            heads_load[i].wait()
            with scope("heads_in"):
                landed(heads_in.at[rows], heads_recv.at[i])
            with scope("own"):
                own = against(factor, jnp.concatenate([heads_in[rows, :], heads_v[rows, :]], axis=1))
                for k in range(group):
                    own_v[i * group + k] = own[:, k * block:(k + 1) * block]

            @pl.when(chip == 0)
            def _():
                for k in range(i * group, (i + 1) * group):
                    pre_out[k] = encode(own_v[k], bound[...])
                    to_right(k).start()

            @pl.when(chip == last)
            def _():
                for k in range(i * group, (i + 1) * group):
                    suf_out[k] = encode(own_v[k], bound[...])
                    to_left(k).start()

        @pl.when(chip == 0)
        def _():
            left_v[...] = jnp.zeros_like(left_v)

        @pl.when(chip == last)
        def _():
            right_v[...] = jnp.zeros_like(right_v)

        acc_own[...] = jnp.zeros_like(acc_own)
        acc_pair[...] = jnp.zeros_like(acc_pair)
        with scope("masters_encode"):
            masters_encode()
        send(mas_top.at[f], pair_mast, give_send.at[0], give_recv.at[0], partner)
        send(mas.at[f], pair_mas, give_send.at[1], give_recv.at[1], partner)

        def output_cotangents():
            ocot_load.wait()
            landed(ocot_in, ocot_recv)

        done = 0
        for at, event in ((13, output_cotangents),):
            at = min(at, steps)
            lax.fori_loop(done, at, step, 0)
            done = at
            with scope(f"event{at}"):
                event()
        lax.fori_loop(done, steps, step, 0)

        with scope("exchange"):
            mine = acc_own[:rank, :] + acc_own[rank:, :]
            pair = acc_pair[:rank, :] + acc_pair[rank:, :]
            top = top_of(pair)
            pair_top[...] = top
            pair_out[...] = encode_even(pair, top)
            top = top_of(mine)
            swap_top[f] = top
            swap[f] = encode_even(mine, top)
            for d in fs_peers:
                there = {"fs": d, "tp": t - 1}
                send(pair_top, swap_top.at[f], mark_send.at[1], mark_recv.at[0], there)
                send(pair_out, swap.at[f], swap_send.at[1], swap_recv.at[0], there)
                send(swap_top.at[f], swap_top.at[f], mark_send.at[0], mark_recv.at[0], {"fs": d})
                send(swap.at[f], swap.at[f], swap_send.at[0], swap_recv.at[0], {"fs": d})
            send(pair_top, swap_top.at[f], mark_send.at[1], mark_recv.at[0], partner)
            send(pair_out, swap.at[f], swap_send.at[1], swap_recv.at[0], partner)
        with scope("back_copy"):
            landed(v_copy.at[pl.ds(0, 2 * v_rows)], back_recv.at[2])
            here = own_rows(v_copy)
            for d in fs_peers:
                send(here, here, copy_send.at[0], copy_recv, {"fs": d})
                send(stage, here, copy_send.at[1], copy_recv, {"fs": d, "tp": t - 1})
        with scope("swap_wait"):
            landed(swap_top.at[pl.ds(0, fs - 1)], mark_recv.at[0])
            landed(swap.at[pl.ds(0, fs - 1)], swap_recv.at[0])

    @pl.when(aide)
    def _():
        pass_right(chip == 0)
        pass_left(chip == last)
        for i, rows in enumerate(pieces):
            heads_load[i].wait()
            send(heads_v.at[rows], heads_in.at[rows], heads_send, heads_recv.at[i], partner)
        send_moments()
        ocot_load.wait()
        send(ocot_v, ocot_in, ocot_send, ocot_recv, partner)
        pass_right((chip > 0) & (chip < near))
        pass_left((chip < last) & (chip >= near))
        with scope("value_load"):
            for load in (vfac_load, vcot_load, vin_load):
                load.wait()
        with scope("value_own"):
            total = jnp.zeros((2 * rank, columns), F32)
            stride = image_v.shape[2]
            value_factor = vfac_v[...].astype(F32).T.astype(BF16)
            for i in range(tokens // stride):
                rows = pl.ds(i * stride, stride)
                two = split(against(value_factor, vcot_v[rows, :]), 0)
                image_v[i] = two
                total = total + jnp.dot(two, vin_v[0, rows, :], preferred_element_type=F32)
            totals_v = [total]
        with scope("value_moments"):
            vm1_load.wait()
            vm2_load.wait()
            landed(v1_v.at[1], gift_recv.at[1])
            landed(v2_v.at[1], gift_recv.at[2])
            for i, local in enumerate((v1_v, v2_v)):
                for h in range(2):
                    top = top_of(local[h])
                    value_momt[f, i, h] = top
                    value_mom[f, i, h] = encode_even(local[h], top)
            for d in fs_peers:
                send(value_momt.at[f], value_momt.at[f], momt_send.at[1], momt_recv.at[1], {"fs": d})
                send(value_mom.at[f], value_mom.at[f], mom_send.at[1], mom_recv.at[1], {"fs": d})
        with scope("gift"):
            landed(vin_v.at[1], gift_recv.at[0])
        with scope("value_pair"):
            total = jnp.zeros((2 * rank, columns), F32)
            for i in range(tokens // stride):
                total = total + jnp.dot(image_v[i], vin_v[1, pl.ds(i * stride, stride), :], preferred_element_type=F32)
            totals_v.append(total)
            for h, total in enumerate(totals_v):
                mine = total[:rank] + total[rank:]
                top = top_of(mine)
                value_top[f, h] = top
                value_swap[f, h] = encode_even(mine, top)
            for d in fs_peers:
                send(value_top.at[f], value_top.at[f], mark_send.at[2], mark_recv.at[1], {"fs": d})
                send(value_swap.at[f], value_swap.at[f], swap_send.at[2], swap_recv.at[1], {"fs": d})
        masters_encode()
        for d in fs_peers:
            send(mas_top.at[f], mas_top.at[f], mast_send.at[0], mast_recv, {"fs": d})
            send(mas.at[f], mas.at[f], mas_send.at[0], mas_recv, {"fs": d})
        with scope("give"):
            landed(pair_mast, give_recv.at[0])
            landed(pair_mas, give_recv.at[1])
        for d in fs_peers:
            there = {"fs": d, "tp": t + 1}
            send(pair_mast, mas_top.at[f], mast_send.at[1], mast_recv, there)
            send(pair_mas, mas.at[f], mas_send.at[1], mas_recv, there)
        pass_right((chip >= near) & (chip < last))
        pass_left((chip > 0) & (chip < near))

        @pl.when(chip == 0)
        def _():
            pl.semaphore_wait(seen.at[1], 1)

        @pl.when(chip == last)
        def _():
            pl.semaphore_wait(seen.at[0], 1)

        with scope("value_swap_wait"):
            landed(value_top.at[pl.ds(0, fs - 1)], mark_recv.at[1])
            landed(value_swap.at[pl.ds(0, fs - 1)], swap_recv.at[1])
        power = jnp.zeros((1, columns), F32)
        for h in range(2):
            whole = decode_even(value_swap[0, h], value_top[0, h])
            for g in range(1, fs):
                whole = whole + decode_even(value_swap[g, h], value_top[g, h])
            proj_v[h] = whole
            power = power + jnp.sum(whole * whole, axis=0, keepdims=True)
        value_sums[chip] = power
        for j in range(1, chips):
            where = {"tp": lax.rem(t + 2 * j, tp)}
            send(value_sums.at[chip], value_sums.at[chip], sum_send.at[0], sum_recv.at[0], where)
        with scope("value_sums_wait"):
            landed(value_sums.at[pl.ds(0, chips - 1)], sum_recv.at[0])
        total = jnp.sum(jnp.sum(value_sums[...], axis=0), axis=1, keepdims=True)
        scale = lax.rsqrt(total / (rank * columns * tp) + 1e-06)
        for h, first_out, second_out in ((0, v_first, v_second), (1, back_first, back_second)):
            scaled = scale * proj_v[h, pl.ds(pl.multiple_of(f * band, band), band), :]
            first_out[...] = 0.9 * v1_v[h] + 0.1 * scaled
            second_out[...] = 0.95 * v2_v[h] + 0.05 * scaled * scaled
        send(back_first, v_first, back_send.at[0], back_recv.at[0], partner)
        send(back_second, v_second, back_send.at[0], back_recv.at[0], partner)
        vmas_load.wait()
        landed(vm_v.at[1], gift_recv.at[3])
        rows = vfac_v[pl.ds(pl.multiple_of(f * v_rows, v_rows), v_rows), :]
        rows = jnp.concatenate([rows, rows], axis=1)
        with scope("mom_wait"):
            landed(value_momt.at[pl.ds(0, fs - 1)], momt_recv.at[1])
            landed(value_mom.at[pl.ds(0, fs - 1)], mom_recv.at[1])
        here = own_rows(v_copy)

        def gathered(i, h):
            return jnp.concatenate([decode_even(value_mom[g, i, h], value_momt[g, i, h]) for g in range(fs)], axis=0)

        for h, step_out, new_out, copy_out in ((1, back_step, back_new, back_copy), (0, v_step, v_new, here)):
            scaled = scale * proj_v[h]
            first_new = 0.9 * gathered(0, h) + 0.1 * scaled
            second_new = 0.95 * gathered(1, h) + 0.05 * scaled * scaled
            direction = split(first_new / (jnp.sqrt(second_new) + 1e-08), 0)
            move = jnp.dot(rows, direction, preferred_element_type=F32)
            fresh = vm_v[h] - 0.002 * move
            step_out[...] = move
            new_out[...] = fresh
            copy_out[...] = fresh.astype(BF16)
            if h == 1:
                send(back_copy, here, back_send.at[2], back_recv.at[2], partner)
                send(back_step, v_step, back_send.at[1], back_recv.at[1], partner)
                send(back_new, v_new, back_send.at[1], back_recv.at[1], partner)
            else:
                send(here, stage, back_send.at[2], back_recv.at[2], partner)
        with scope("swap_wait"):
            landed(swap_top, mark_recv.at[0])
            landed(swap, swap_recv.at[0])

    with scope("sum_out"):
        whole = decode_even(swap[0], swap_top[0])
        for g in range(1, fs):
            whole = whole + decode_even(swap[g], swap_top[g])
        o_all[...] = whole
        sums[t] = jnp.sum(whole * whole, axis=0, keepdims=True)
        for j in range(1, tp):
            send(sums.at[t], sums.at[t], sum_send.at[1], sum_recv.at[1], {"tp": lax.rem(t + j, tp)})
    with scope("masters_wait"):
        masters_end()
    with scope("mom_wait"):
        landed(mom_top.at[pl.ds(0, fs - 1)], momt_recv.at[0])
        landed(mom.at[pl.ds(0, fs - 1)], mom_recv.at[0])
        for i, whole in ((0, o1_all), (1, o2_all)):
            for g in range(fs):
                whole[pl.ds(g * band, band), :] = decode_even(mom[g, i], mom_top[g, i])
        left_here(mom_top.at[pl.ds(0, fs - 1)], momt_send.at[0])
        left_here(mom.at[pl.ds(0, fs - 1)], mom_send.at[0])

    with scope("drain"):
        copies = v_copy.at[pl.ds(0, (fs - 1) * v_rows)]

        @pl.when(aide)
        def _():
            left_here(heads_in, heads_send)
            left_here(ocot_in, ocot_send)
            left_here(value_swap.at[pl.ds(0, fs - 1)], swap_send.at[2])
            left_here(value_top.at[pl.ds(0, fs - 1)], mark_send.at[2])
            left_here(value_momt.at[pl.ds(0, fs - 1)], momt_send.at[1])
            left_here(value_mom.at[pl.ds(0, fs - 1)], mom_send.at[1])
            left_here(value_sums.at[pl.ds(0, chips - 1)], sum_send.at[0])
            for i in range(2):
                left_here(mas.at[pl.ds(0, fs - 1)], mas_send.at[i])
                left_here(mas_top.at[pl.ds(0, fs - 1)], mast_send.at[i])
            left_here(v1_v, back_send.at[0])
            left_here(vm_v, back_send.at[1])
            left_here(v_copy.at[pl.ds(0, 2 * v_rows)], back_send.at[2])

        @pl.when(hub)
        def _():
            for i, ref in enumerate((vin_v, v1_v, v2_v, vm_v)):
                left_here(ref.at[1], gift_send.at[i])
            left_here(pair_mast, give_send.at[0])
            left_here(pair_mas, give_send.at[1])
            left_here(swap.at[pl.ds(0, fs - 1)], swap_send.at[0])
            left_here(swap_top.at[pl.ds(0, fs - 1)], mark_send.at[0])
            left_here(swap, swap_send.at[1])
            left_here(swap_top, mark_send.at[1])
            landed(v1_v, back_recv.at[0])
            landed(vm_v, back_recv.at[1])
            left_here(copies, copy_send.at[0])
            left_here(copies, copy_send.at[1])

        @pl.when(hub & (chip < last))
        def _():
            left_here(pre_out, pre_send)

        @pl.when(hub & (chip > 0))
        def _():
            left_here(suf_out, suf_send)

    with scope("copy_wait"):
        landed(copies, copy_recv)
    with scope("sums_wait"):
        landed(sums.at[pl.ds(0, tp - 1)], sum_recv.at[1])
        totals[...] = jnp.sum(sums[...], axis=0)
        left_here(sums.at[pl.ds(0, tp - 1)], sum_send.at[1])


def finish_kernel(
    fs, tp,
    o_all, o1_all, o2_all, om_all, totals, ofac, omas, om1, om2, v_step, v_new, v_copy, v_first, v_second,
    v_step_out, v_new_out, v_copy_out, v_first_out, v_second_out,
    o_step_out, o_new_out, o_copy_out, o_first_out, o_second_out,
    step_v, new_v, copy_v, first_v, second_v, out_sem,
):
    f = lax.axis_index("fs")
    puts = []

    def put(src, dst):
        copy = pltpu.make_async_copy(src, dst, out_sem.at[len(puts)])
        copy.start()
        puts.append(copy)

    for src, dst in (
        (v_step, v_step_out), (v_new, v_new_out), (v_copy, v_copy_out), (v_first, v_first_out), (v_second, v_second_out),
    ):
        put(src, dst)
    rank, columns = o1_all.shape
    band = rank // fs
    total = jnp.sum(totals[...], axis=1, keepdims=True)
    scale = lax.rsqrt(total / (rank * columns * tp) + 1e-06)

    def moments(proj, first, second):
        scaled = scale * proj
        first_new = 0.9 * first + 0.1 * scaled
        second_new = 0.95 * second + 0.05 * scaled * scaled
        return first_new, second_new

    own_band = pl.ds(pl.multiple_of(f * band, band), band)
    first_v[...], second_v[...] = moments(o_all[own_band, :], om1[...], om2[...])
    put(first_v, o_first_out)
    put(second_v, o_second_out)
    first_new, second_new = moments(o_all[...], o1_all[...], o2_all[...])
    direction = split(first_new / (jnp.sqrt(second_new) + 1e-08), 0)

    def step_of(rows):
        left = ofac[rows, :]
        return jnp.dot(jnp.concatenate([left, left], axis=1), direction, preferred_element_type=F32)

    count = step_v.shape[0]
    own = pl.ds(pl.multiple_of(f * count, count), count)
    move = step_of(own)
    step_v[...] = move
    put(step_v, o_step_out)
    new_v[...] = omas[...] - 0.002 * move
    put(new_v, o_new_out)
    for i in range(fs):
        rows = pl.ds(i * count, count)
        copy_v[rows, :] = (om_all[rows, :] - 0.002 * step_of(rows)).astype(BF16)
        put(copy_v.at[rows], o_copy_out.at[rows])
    for copy in puts:
        copy.wait()


def on_device(vin, vcot, vfac, vmas, vm1, vm2, heads, ocot, ofac, omas, om1, om2):
    fs = lax.axis_size("fs")
    tp = lax.axis_size("tp")
    rank = vfac.shape[1]
    band = rank // fs
    columns = vin.shape[1]
    tokens, width = heads.shape
    block = 128
    blocks = tokens // block
    stride = 256 if tokens % 256 == 0 else tokens

    def twice(array):
        return pltpu.VMEM((2, *array.shape), array.dtype)

    def like(array):
        return pltpu.VMEM(array.shape, array.dtype)

    def shape(*dims, kind=F32):
        return jax.ShapeDtypeStruct(dims, kind)

    def wide(*dims):
        return pltpu.VMEM(dims, F32)

    def coded():
        return pltpu.VMEM((blocks, rank, block), BF16)

    dma = pltpu.SemaphoreType.DMA
    v_rows, o_rows = vmas.shape[0], omas.shape[0]
    gathered = pl.pallas_call(
        functools.partial(gather_kernel, fs, tp),
        out_shape=(
            shape(rank, columns), shape(rank, columns), shape(rank, columns), shape(fs * o_rows, columns),
            shape(1, columns),
            shape(v_rows, columns), shape(v_rows, columns), shape(fs * v_rows, columns, kind=BF16),
            shape(band, columns), shape(band, columns),
        ),
        in_specs=[HBM] * 12,
        out_specs=(VMEM,) * 10,
        scratch_shapes=[
            like(vfac), like(ofac), twice(vin), like(vcot), pltpu.VMEM((tokens // stride, 2 * rank, stride), BF16),
            like(heads), like(heads), like(ocot), like(ocot), twice(vm1), twice(vm2), twice(vmas), like(omas), like(om1), like(om2),
            wide(blocks, rank, block), wide(blocks, rank, block), wide(blocks, rank, block),
            coded(), coded(), coded(), coded(), wide(1, block),
            wide(2 * rank, columns), wide(2 * rank, columns),
            pltpu.VMEM((rank, columns), BF16), wide(1, columns),
            pltpu.VMEM((fs, rank, columns), BF16), wide(fs, 1, columns),
            pltpu.VMEM((fs, 2, rank, columns), BF16), wide(fs, 2, 1, columns),
            wide(2, rank, columns),
            pltpu.VMEM((fs, 2, band, columns), BF16), wide(fs, 2, 1, columns),
            pltpu.VMEM((fs, 2, 2, band, columns), BF16), wide(fs, 2, 2, 1, columns), wide(tp, 1, columns), wide(tp // 2, 1, columns),
            pltpu.VMEM((fs, o_rows, columns), BF16), wide(fs, 1, columns),
            pltpu.VMEM((o_rows, columns), BF16), wide(1, columns),
            wide(band, columns), wide(band, columns), wide(v_rows, columns), wide(v_rows, columns),
            pltpu.VMEM((v_rows, columns), BF16), pltpu.VMEM((v_rows, columns), BF16),
            dma((10 + HEADS_PIECES,)), dma, dma((HEADS_PIECES,)), dma, dma, dma((4,)), dma((4,)),
            dma, dma((blocks,)), dma, dma((blocks,)),
            dma((3,)), dma((2,)), dma((3,)), dma((2,)), dma((2,)), dma((2,)), pltpu.SemaphoreType.REGULAR((2,)),
            dma((2,)), dma((2,)), dma((2,)), dma((2,)), dma((2,)), dma, dma((2,)), dma, dma((2,)), dma((2,)), dma((3,)), dma((3,)), dma((2,)), dma,
        ],
        compiler_params=pltpu.CompilerParams(
            collective_id=0, has_side_effects=True, vmem_limit_bytes=32 * 1024 * 1024
        ),
    )(*(pltpu.with_memory_space_constraint(a, pltpu.HBM) for a in (
        vin, vcot, vfac, vmas, vm1, vm2, heads, ocot, ofac, omas, om1, om2
    )))
    o_all, o1_all, o2_all, om_all, totals, *values = gathered

    return pl.pallas_call(
        functools.partial(finish_kernel, fs, tp),
        out_shape=(
            shape(v_rows, columns), shape(v_rows, columns), shape(fs * v_rows, columns, kind=BF16),
            shape(band, columns), shape(band, columns),
            shape(o_rows, columns), shape(o_rows, columns), shape(fs * o_rows, columns, kind=BF16),
            shape(band, columns), shape(band, columns),
        ),
        in_specs=[VMEM] * 14,
        out_specs=(HBM,) * 10,
        scratch_shapes=[
            wide(o_rows, columns), wide(o_rows, columns), pltpu.VMEM((fs * o_rows, columns), BF16),
            wide(band, columns), wide(band, columns), dma((9 + fs,)),
        ],
        compiler_params=pltpu.CompilerParams(vmem_limit_bytes=24 * 1024 * 1024),
    )(o_all, o1_all, o2_all, om_all, totals, ofac, omas, om1, om2, *values)


def solution(mesh):
    both = P("fs", "tp")
    in_specs = (both, P("fs", None), P(), both, both, both, both, both, P(), both, both, both)
    out_specs = (
        both, both, P(None, "tp"), both, both, both, both, P(None, "tp"), both, both,
    )
    return jax.shard_map(
        on_device, mesh=mesh, in_specs=in_specs, out_specs=out_specs, check_vma=False
    )
```

time: 33.3 us -> 30.5 us (0.916)
  Pallas kernels: 32.5 us -> 29.6 us
    pallas_call x1, Pallas kernels: 31 us -> 28.1 us  [on_device(): pl.pallas_call(functools.partial(gather_kernel, fs, tp), out_shape=(shape...]
where the time goes in v3:
time: 30.5 us; the launch traced here: 30.3 us
  Pallas kernels  29.6 us (97%)
  between operations  0.72 us (2%)
    pallas_call x1, Pallas kernels, on_device(): pl.pallas_call(functools.partial(gather_kernel, fs, tp), out_shape=(shape...  28.1 us
    pallas_call x1, Pallas kernels, on_device(): pl.pallas_call(functools.partial(finish_kernel, fs, tp), out_shape=(shape...  1.45 us

profile of v3, /device:TPU:0, one launch (start us, length us, event | category | flops | bytes accessed | tf_op | source)
XLA Modules:
  0.0 30.3 jit_solution(17980861035828273130)
XLA Ops:
  0.6 0.0 copy-start.3
  0.7 0.0 copy-start.2
  0.7 0.0 copy-start.1
  0.7 0.0 copy-start
  0.7 28.1 %shard_map.195 = (f32[128,256]{1,0:T(8,128)S(1)}, f32[128,256]{1,0:T(8,128)S(1)}, f32[128,256]{1,0:T(8,128)S(1)}, f32[1024,256]{1,0:T(8,128)S(1)}, f32[1,256]{1,...) custom-call(bf16[2048,256]{1,0:T(8,128)(2,1)} %vin.1, ...), custom_call_target="tpu_custom_call" | custom-call | tf_op jit(solution)/shard_map/pallas_call | solution.py:645
  28.8 0.0 copy-done.3
  28.8 0.0 copy-done.2
  28.8 0.0 copy-done.1
  28.8 0.0 copy-done
  28.9 1.4 %shard_map.196 = (f32[128,256]{1,0:T(8,128)}, f32[128,256]{1,0:T(8,128)}, bf16[512,256]{1,0:T(8,128)(2,1)}, f32[32,256]{1,0:T(8,128)}, f32[32,256]{1,0:T(8,128)}...) custom-call(f32[128,256]{1,0:T(8,128)S(1)} %get-tuple-element.20.o_a, ...), custom_call_target="tpu_custom_call" | custom-call | tf_op jit(solution)/shard_map/pallas_call | solution.py:684
Async XLA Ops:
  0.6 28.2 %copy-start.3 = (f32[32,256]{1,0:T(8,128)S(1)}, f32[32,256]{1,0:T(8,128)}, u32[]{:S(2)}) copy-start(f32[32,256]{1,0:T(8,128)} %om2.3) | copy-start | bytes 98308
  0.7 28.2 %copy-start.2 = (f32[32,256]{1,0:T(8,128)S(1)}, f32[32,256]{1,0:T(8,128)}, u32[]{:S(2)}) copy-start(f32[32,256]{1,0:T(8,128)} %om1.3) | copy-start | bytes 98308
  0.7 28.2 %copy-start.1 = (f32[256,256]{1,0:T(8,128)S(1)}, f32[256,256]{1,0:T(8,128)}, u32[]{:S(2)}) copy-start(f32[256,256]{1,0:T(8,128)} %omas.3) | copy-start | bytes 786436
  0.7 28.2 %copy-start = (bf16[1024,128]{1,0:T(8,128)(2,1)S(1)}, bf16[1024,128]{1,0:T(8,128)(2,1)}, u32[]{:S(2)}) copy-start(bf16[1024,128]{1,0:T(8,128)(2,1)} %ofac.3) | copy-start | bytes 786436

commit v4 on v3

--- a/solution.py
+++ b/solution.py
@@ -13,13 +13,12 @@
 VMEM = pl.BlockSpec(memory_space=pltpu.VMEM)
 BF16 = jnp.bfloat16
 F32 = jnp.float32
-PRE = 5
+PRE = 6
 SUF = 7
 LEVELS = 252.0
 POWER = 7
 PEAK = 240000.0
 HEADS_BOUND = 6.0
-HEADS_PIECES = 4
 
 
 def split(wide, axis):
@@ -57,17 +56,24 @@
     return jnp.max(jnp.abs(x), axis=0, keepdims=True) * 1.02 + 1e-30
 
 
+def growing(blocks):
+    sizes = [1]
+    while sum(sizes) < blocks:
+        sizes.append(min(sum(sizes), blocks - sum(sizes)))
+    return sizes
+
+
 def gather_kernel(
     fs, tp,
     vin, vcot, vfac, vmas, vm1, vm2, heads, ocot, ofac, omas, om1, om2,
     o_all, o1_all, o2_all, om_all, totals, v_step, v_new, v_copy, v_first, v_second,
     vfac_v, ofac_v, vin_v, vcot_v, image_v, heads_v, heads_in, ocot_v, ocot_in, v1_v, v2_v, vm_v, om_v, o1_v, o2_v,
     own_v, left_v, right_v, pre_in, pre_out, suf_in, suf_out, bound, acc_own, acc_pair,
-    pair_out, pair_top, swap, swap_top, value_swap, value_top, proj_v, mom, mom_top, value_mom, value_momt, sums, value_sums, mas, mas_top,
-    pair_mas, pair_mast, back_first, back_second, back_step, back_new, back_copy, stage,
-    load_sem, heads_send, heads_recv, ocot_send, ocot_recv, gift_send, gift_recv, pre_send, pre_recv, suf_send, suf_recv,
-    swap_send, swap_recv, mark_send, mark_recv, sum_send, sum_recv, seen,
-    mom_send, mom_recv, momt_send, momt_recv, mas_send, mas_recv, mast_send, mast_recv, give_send, give_recv, back_send, back_recv, copy_send, copy_recv,
+    part, part_out, part_top, part_in, part_top_in, stage, value_swap, value_top, proj_v, mom, mom_top, value_mom, value_momt, sums, value_sums, mas, mas_top,
+    pair_mas, pair_mast, back_first, back_second, back_step, back_new, back_copy, value_mas, value_mast, move_v,
+    load_sem, heads_recv, ocot_recv, gift_send, pre_send, pre_recv, suf_send, suf_recv,
+    part_send, part_recv, mark_send, mark_recv, all_send, all_recv, sum_send, sum_recv, seen,
+    mom_send, mom_recv, momt_send, momt_recv, mas_recv, mast_recv, give_send, back_recv, copy_recv,
 ):
     f = lax.axis_index("fs")
     t = lax.axis_index("tp")
@@ -82,13 +88,23 @@
     blocks, _, block = own_v.shape
     o_rows = omas.shape[0]
     v_rows = vmas.shape[0]
-    piece = tokens // HEADS_PIECES
     scope = jax.named_scope
     hub = core == 1
     aide = core == 0
     at_last = (last - chip + last) // chips
     at_first = (chip + last) // chips
 
+    spare = iter([sems.at[i] for sems in (pre_recv, suf_recv) for i in range(blocks)])
+    heads_send, ocot_send = next(spare), next(spare)
+    gift_recv = [next(spare) for _ in range(4)]
+    value_swap_send, value_swap_recv, value_mark_send, value_mark_recv = (next(spare) for _ in range(4))
+    value_sum_send, value_sum_recv = next(spare), next(spare)
+    value_mom_send, value_mom_recv, value_momt_send, value_momt_recv = (next(spare) for _ in range(4))
+    mas_send, mast_send, give_recv = ([next(spare) for _ in range(2)] for _ in range(3))
+    back_send = [next(spare) for _ in range(2)]
+    copy_send = next(spare)
+    value_mas_send, value_mas_recv, value_mast_send, value_mast_recv = (next(spare) for _ in range(4))
+
     fs_peers = [3 - f, f + 1 - 2 * (f % 2), lax.rem(f + 2, fs)] if fs == 4 else [lax.rem(f + j, fs) for j in range(1, fs)]
     partner = {"tp": chip * 2 + (1 - core)}
     right = {"tp": lax.rem(t + 2, tp)}
@@ -98,24 +114,28 @@
         rows = ref.shape[0] // fs
         return ref.at[pl.ds(pl.multiple_of(f * rows, rows), rows)]
 
-    pieces = [pl.ds(i * piece, piece) for i in range(HEADS_PIECES)]
-    count = HEADS_PIECES
+    sizes = growing(blocks)
+    count = len(sizes)
+    starts = [sum(sizes[:i]) for i in range(count)]
+    pieces = [pl.ds(a * block, n * block) for a, n in zip(starts, sizes)]
 
     def loading(i, src, dst):
         return pltpu.make_async_copy(src, dst, load_sem.at[i])
 
     heads_load = [loading(i, heads.at[rows], heads_v.at[rows]) for i, rows in enumerate(pieces)]
     om1_load = loading(count, om1, o1_v)
-    om2_load = loading(count + 1, om2, o2_v)
+    om2_load = loading(count, om2, o2_v)
+    om12_load = loading(count, om_v.at[pl.ds(0, 2 * band)], om_v.at[pl.ds(0, 2 * band)])
     omas_load = loading(count + 2, omas, om_v)
     ocot_load = loading(count + 3, ocot, ocot_v)
     ofac_load = loading(count + 4, ofac, ofac_v)
     vfac_load = loading(count + 4, vfac, vfac_v)
     vcot_load = loading(count + 5, vcot, vcot_v)
     vin_load = loading(count + 6, vin, vin_v.at[0])
-    vm1_load = loading(count + 7, vm1, v1_v.at[0])
-    vm2_load = loading(count + 8, vm2, v2_v.at[0])
-    vmas_load = loading(count + 9, vmas, vm_v.at[0])
+    vm1_load = loading(count + 1, vm1, v1_v.at[0])
+    vm2_load = loading(count + 1, vm2, v2_v.at[0])
+    vm12_load = loading(count + 1, v1_v, v1_v)
+    vmas_load = loading(count + 7, vmas, vm_v.at[0])
 
     heads_load[0].start()
 
@@ -133,7 +153,7 @@
 
     @pl.when(aide)
     def _():
-        for load in (ocot_load, vfac_load, vcot_load, vin_load, omas_load, vm1_load, vm2_load, vmas_load):
+        for load in (omas_load, ocot_load, vfac_load, vcot_load, vin_load, vm1_load, vm2_load, vmas_load):
             load.start()
 
     barrier = pltpu.get_barrier_semaphore()
@@ -205,14 +225,14 @@
         return remote(suf_out.at[k], suf_in.at[k], suf_send, suf_recv.at[k], left)
 
     def send_moments():
-        for i, (load, local) in enumerate(((om1_load, o1_v), (om2_load, o2_v))):
-            load.wait()
+        om12_load.wait()
+        for i, local in enumerate((o1_v, o2_v)):
             top = top_of(local[...])
             mom_top[f, i] = top
             mom[f, i] = encode_even(local[...], top)
         for d in fs_peers:
-            send(mom_top.at[f], mom_top.at[f], momt_send.at[0], momt_recv.at[0], {"fs": d})
-            send(mom.at[f], mom.at[f], mom_send.at[0], mom_recv.at[0], {"fs": d})
+            send(mom_top.at[f], mom_top.at[f], momt_send, momt_recv, {"fs": d})
+            send(mom.at[f], mom.at[f], mom_send, mom_recv, {"fs": d})
 
     def masters_encode():
         omas_load.wait()
@@ -273,7 +293,7 @@
     @pl.when(hub)
     def _():
         for i, (src, dst) in enumerate(((vin, vin_v), (vm1, v1_v), (vm2, v2_v), (vmas, vm_v))):
-            send(src, dst.at[1], gift_send.at[i], gift_recv.at[i], partner)
+            send(src, dst.at[1], gift_send.at[i], gift_recv[i], partner)
         send_moments()
         with scope("factor"):
             ofac_load.wait()
@@ -281,25 +301,24 @@
             top = jnp.max(reach, axis=1, keepdims=True) * (1.02 * HEADS_BOUND) + 1e-30
             bound[...] = jnp.broadcast_to(top, bound.shape)
             factor = jnp.concatenate([factor_of(t - 1), factor_of(t)], axis=1)
-        group = blocks // HEADS_PIECES
         for i, rows in enumerate(pieces):
             heads_load[i].wait()
             with scope("heads_in"):
                 landed(heads_in.at[rows], heads_recv.at[i])
             with scope("own"):
                 own = against(factor, jnp.concatenate([heads_in[rows, :], heads_v[rows, :]], axis=1))
-                for k in range(group):
-                    own_v[i * group + k] = own[:, k * block:(k + 1) * block]
+                for k in range(sizes[i]):
+                    own_v[starts[i] + k] = own[:, k * block:(k + 1) * block]
 
             @pl.when(chip == 0)
             def _():
-                for k in range(i * group, (i + 1) * group):
+                for k in range(starts[i], starts[i] + sizes[i]):
                     pre_out[k] = encode(own_v[k], bound[...])
                     to_right(k).start()
 
             @pl.when(chip == last)
             def _():
-                for k in range(i * group, (i + 1) * group):
+                for k in range(starts[i], starts[i] + sizes[i]):
                     suf_out[k] = encode(own_v[k], bound[...])
                     to_left(k).start()
 
@@ -315,8 +334,8 @@
         acc_pair[...] = jnp.zeros_like(acc_pair)
         with scope("masters_encode"):
             masters_encode()
-        send(mas_top.at[f], pair_mast, give_send.at[0], give_recv.at[0], partner)
-        send(mas.at[f], pair_mas, give_send.at[1], give_recv.at[1], partner)
+        send(mas_top.at[f], pair_mast, give_send.at[0], give_recv[0], partner)
+        send(mas.at[f], pair_mas, give_send.at[1], give_recv[1], partner)
 
         def output_cotangents():
             ocot_load.wait()
@@ -334,29 +353,52 @@
         with scope("exchange"):
             mine = acc_own[:rank, :] + acc_own[rank:, :]
             pair = acc_pair[:rank, :] + acc_pair[rank:, :]
-            top = top_of(pair)
-            pair_top[...] = top
-            pair_out[...] = encode_even(pair, top)
-            top = top_of(mine)
-            swap_top[f] = top
-            swap[f] = encode_even(mine, top)
+            for h, whole in enumerate((pair, mine)):
+                part[h] = whole
+                top = top_of(whole)
+                part_top[h] = top
+                coded_part = encode_even(whole, top)
+                for g in range(fs):
+                    part_out[g, h] = coded_part[g * band:(g + 1) * band]
             for d in fs_peers:
-                there = {"fs": d, "tp": t - 1}
-                send(pair_top, swap_top.at[f], mark_send.at[1], mark_recv.at[0], there)
-                send(pair_out, swap.at[f], swap_send.at[1], swap_recv.at[0], there)
-                send(swap_top.at[f], swap_top.at[f], mark_send.at[0], mark_recv.at[0], {"fs": d})
-                send(swap.at[f], swap.at[f], swap_send.at[0], swap_recv.at[0], {"fs": d})
-            send(pair_top, swap_top.at[f], mark_send.at[1], mark_recv.at[0], partner)
-            send(pair_out, swap.at[f], swap_send.at[1], swap_recv.at[0], partner)
-        with scope("back_copy"):
-            landed(v_copy.at[pl.ds(0, 2 * v_rows)], back_recv.at[2])
-            here = own_rows(v_copy)
+                send(part_top, part_top_in.at[f], mark_send, mark_recv, {"fs": d})
+                send(part_out.at[d], part_in.at[f], part_send, part_recv, {"fs": d})
+        with scope("part_wait"):
+            landed(part_top_in.at[pl.ds(0, fs - 1)], mark_recv)
+            landed(part_in.at[pl.ds(0, fs - 1)], part_recv)
+        with scope("sum_out"):
+            power = jnp.zeros((1, columns), F32)
+            for h, out in ((0, stage), (1, own_rows(o_all))):
+                whole = part[h, pl.ds(pl.multiple_of(f * band, band), band), :]
+                for d in fs_peers:
+                    whole = whole + decode_even(part_in[d, h], part_top_in[d, h])
+                out[...] = whole
+                power = power + jnp.sum(whole * whole, axis=0, keepdims=True)
+            me = f * chips + chip
+            sums[me] = power
+
+            def spread(i, j, c):
+                where = {"fs": lax.rem(f + i, fs), "tp": 2 * lax.rem(chip + j, chips) + c}
+                send(sums.at[me], sums.at[me], sum_send, sum_recv, where)
+
+            if fs * chips <= 16:
+                for i in range(fs - 1, -1, -1):
+                    for j in range(chips):
+                        for c in range(2):
+                            if (i, j, c) != (0, 0, 1):
+                                spread(i, j, c)
+            else:
+                def spread_one(k, _):
+                    spread(k // (2 * chips), (k // 2) % chips, k % 2)
+                    return 0
+
+                spread(0, 0, 0)
+                lax.fori_loop(2, 2 * fs * chips, spread_one, 0)
+            here = own_rows(o_all)
             for d in fs_peers:
-                send(here, here, copy_send.at[0], copy_recv, {"fs": d})
-                send(stage, here, copy_send.at[1], copy_recv, {"fs": d, "tp": t - 1})
-        with scope("swap_wait"):
-            landed(swap_top.at[pl.ds(0, fs - 1)], mark_recv.at[0])
-            landed(swap.at[pl.ds(0, fs - 1)], swap_recv.at[0])
+                send(here, here, all_send.at[0], all_recv, {"fs": d})
+                send(stage, here, all_send.at[1], all_recv, {"fs": d, "tp": t - 1})
+            send(stage, here, all_send.at[1], all_recv, partner)
 
     @pl.when(aide)
     def _():
@@ -366,6 +408,11 @@
             heads_load[i].wait()
             send(heads_v.at[rows], heads_in.at[rows], heads_send, heads_recv.at[i], partner)
         send_moments()
+        with scope("masters_encode"):
+            masters_encode()
+        for d in fs_peers:
+            send(mas_top.at[f], mas_top.at[f], mast_send[0], mast_recv, {"fs": d})
+            send(mas.at[f], mas.at[f], mas_send[0], mas_recv, {"fs": d})
         ocot_load.wait()
         send(ocot_v, ocot_in, ocot_send, ocot_recv, partner)
         pass_right((chip > 0) & (chip < near))
@@ -383,21 +430,8 @@
                 image_v[i] = two
                 total = total + jnp.dot(two, vin_v[0, rows, :], preferred_element_type=F32)
             totals_v = [total]
-        with scope("value_moments"):
-            vm1_load.wait()
-            vm2_load.wait()
-            landed(v1_v.at[1], gift_recv.at[1])
-            landed(v2_v.at[1], gift_recv.at[2])
-            for i, local in enumerate((v1_v, v2_v)):
-                for h in range(2):
-                    top = top_of(local[h])
-                    value_momt[f, i, h] = top
-                    value_mom[f, i, h] = encode_even(local[h], top)
-            for d in fs_peers:
-                send(value_momt.at[f], value_momt.at[f], momt_send.at[1], momt_recv.at[1], {"fs": d})
-                send(value_mom.at[f], value_mom.at[f], mom_send.at[1], mom_recv.at[1], {"fs": d})
         with scope("gift"):
-            landed(vin_v.at[1], gift_recv.at[0])
+            landed(vin_v.at[1], gift_recv[0])
         with scope("value_pair"):
             total = jnp.zeros((2 * rank, columns), F32)
             for i in range(tokens // stride):
@@ -409,19 +443,37 @@
                 value_top[f, h] = top
                 value_swap[f, h] = encode_even(mine, top)
             for d in fs_peers:
-                send(value_top.at[f], value_top.at[f], mark_send.at[2], mark_recv.at[1], {"fs": d})
-                send(value_swap.at[f], value_swap.at[f], swap_send.at[2], swap_recv.at[1], {"fs": d})
-        masters_encode()
-        for d in fs_peers:
-            send(mas_top.at[f], mas_top.at[f], mast_send.at[0], mast_recv, {"fs": d})
-            send(mas.at[f], mas.at[f], mas_send.at[0], mas_recv, {"fs": d})
+                send(value_top.at[f], value_top.at[f], value_mark_send, value_mark_recv, {"fs": d})
+                send(value_swap.at[f], value_swap.at[f], value_swap_send, value_swap_recv, {"fs": d})
+        with scope("value_moments"):
+            vm12_load.wait()
+            landed(v1_v.at[1], gift_recv[1])
+            landed(v2_v.at[1], gift_recv[2])
+            for i, local in enumerate((v1_v, v2_v)):
+                for h in range(2):
+                    top = top_of(local[h])
+                    value_momt[f, i, h] = top
+                    value_mom[f, i, h] = encode_even(local[h], top)
+            for d in fs_peers:
+                send(value_momt.at[f], value_momt.at[f], value_momt_send, value_momt_recv, {"fs": d})
+                send(value_mom.at[f], value_mom.at[f], value_mom_send, value_mom_recv, {"fs": d})
         with scope("give"):
-            landed(pair_mast, give_recv.at[0])
-            landed(pair_mas, give_recv.at[1])
+            landed(pair_mast, give_recv[0])
+            landed(pair_mas, give_recv[1])
         for d in fs_peers:
             there = {"fs": d, "tp": t + 1}
-            send(pair_mast, mas_top.at[f], mast_send.at[1], mast_recv, there)
-            send(pair_mas, mas.at[f], mas_send.at[1], mas_recv, there)
+            send(pair_mast, mas_top.at[f], mast_send[1], mast_recv, there)
+            send(pair_mas, mas.at[f], mas_send[1], mas_recv, there)
+        with scope("value_masters"):
+            vmas_load.wait()
+            landed(vm_v.at[1], gift_recv[3])
+            for h in range(2):
+                top = top_of(vm_v[h])
+                value_mast[f, h] = top
+                value_mas[f, h] = encode_even(vm_v[h], top)
+            for d in fs_peers:
+                send(value_mast.at[f], value_mast.at[f], value_mast_send, value_mast_recv, {"fs": d})
+                send(value_mas.at[f], value_mas.at[f], value_mas_send, value_mas_recv, {"fs": d})
         pass_right((chip >= near) & (chip < last))
         pass_left((chip > 0) & (chip < near))
 
@@ -434,8 +486,8 @@
             pl.semaphore_wait(seen.at[0], 1)
 
         with scope("value_swap_wait"):
-            landed(value_top.at[pl.ds(0, fs - 1)], mark_recv.at[1])
-            landed(value_swap.at[pl.ds(0, fs - 1)], swap_recv.at[1])
+            landed(value_top.at[pl.ds(0, fs - 1)], value_mark_recv)
+            landed(value_swap.at[pl.ds(0, fs - 1)], value_swap_recv)
         power = jnp.zeros((1, columns), F32)
         for h in range(2):
             whole = decode_even(value_swap[0, h], value_top[0, h])
@@ -446,86 +498,87 @@
         value_sums[chip] = power
         for j in range(1, chips):
             where = {"tp": lax.rem(t + 2 * j, tp)}
-            send(value_sums.at[chip], value_sums.at[chip], sum_send.at[0], sum_recv.at[0], where)
+            send(value_sums.at[chip], value_sums.at[chip], value_sum_send, value_sum_recv, where)
         with scope("value_sums_wait"):
-            landed(value_sums.at[pl.ds(0, chips - 1)], sum_recv.at[0])
+            landed(value_sums.at[pl.ds(0, chips - 1)], value_sum_recv)
         total = jnp.sum(jnp.sum(value_sums[...], axis=0), axis=1, keepdims=True)
         scale = lax.rsqrt(total / (rank * columns * tp) + 1e-06)
         for h, first_out, second_out in ((0, v_first, v_second), (1, back_first, back_second)):
             scaled = scale * proj_v[h, pl.ds(pl.multiple_of(f * band, band), band), :]
             first_out[...] = 0.9 * v1_v[h] + 0.1 * scaled
             second_out[...] = 0.95 * v2_v[h] + 0.05 * scaled * scaled
-        send(back_first, v_first, back_send.at[0], back_recv.at[0], partner)
-        send(back_second, v_second, back_send.at[0], back_recv.at[0], partner)
-        vmas_load.wait()
-        landed(vm_v.at[1], gift_recv.at[3])
-        rows = vfac_v[pl.ds(pl.multiple_of(f * v_rows, v_rows), v_rows), :]
+        send(back_first, v_first, back_send[0], back_recv.at[0], partner)
+        send(back_second, v_second, back_send[0], back_recv.at[0], partner)
+        rows = vfac_v[...]
         rows = jnp.concatenate([rows, rows], axis=1)
         with scope("mom_wait"):
-            landed(value_momt.at[pl.ds(0, fs - 1)], momt_recv.at[1])
-            landed(value_mom.at[pl.ds(0, fs - 1)], mom_recv.at[1])
-        here = own_rows(v_copy)
+            landed(value_momt.at[pl.ds(0, fs - 1)], value_momt_recv)
+            landed(value_mom.at[pl.ds(0, fs - 1)], value_mom_recv)
+            landed(value_mast.at[pl.ds(0, fs - 1)], value_mast_recv)
+            landed(value_mas.at[pl.ds(0, fs - 1)], value_mas_recv)
 
         def gathered(i, h):
             return jnp.concatenate([decode_even(value_mom[g, i, h], value_momt[g, i, h]) for g in range(fs)], axis=0)
 
-        for h, step_out, new_out, copy_out in ((1, back_step, back_new, back_copy), (0, v_step, v_new, here)):
+        for h, step_out, new_out, copy_out in ((1, back_step, back_new, back_copy), (0, v_step, v_new, v_copy)):
             scaled = scale * proj_v[h]
             first_new = 0.9 * gathered(0, h) + 0.1 * scaled
             second_new = 0.95 * gathered(1, h) + 0.05 * scaled * scaled
             direction = split(first_new / (jnp.sqrt(second_new) + 1e-08), 0)
-            move = jnp.dot(rows, direction, preferred_element_type=F32)
-            fresh = vm_v[h] - 0.002 * move
+            move_v[...] = jnp.dot(rows, direction, preferred_element_type=F32)
+            move = own_rows(move_v)[...]
             step_out[...] = move
-            new_out[...] = fresh
-            copy_out[...] = fresh.astype(BF16)
+            new_out[...] = vm_v[h] - 0.002 * move
+            for g in range(fs):
+                these = pl.ds(g * v_rows, v_rows)
+                old = decode_even(value_mas[g, h], value_mast[g, h])
+                copy_out[these, :] = (old - 0.002 * move_v[these, :]).astype(BF16)
             if h == 1:
-                send(back_copy, here, back_send.at[2], back_recv.at[2], partner)
-                send(back_step, v_step, back_send.at[1], back_recv.at[1], partner)
-                send(back_new, v_new, back_send.at[1], back_recv.at[1], partner)
-            else:
-                send(here, stage, back_send.at[2], back_recv.at[2], partner)
-        with scope("swap_wait"):
-            landed(swap_top, mark_recv.at[0])
-            landed(swap, swap_recv.at[0])
-
-    with scope("sum_out"):
-        whole = decode_even(swap[0], swap_top[0])
-        for g in range(1, fs):
-            whole = whole + decode_even(swap[g], swap_top[g])
-        o_all[...] = whole
-        sums[t] = jnp.sum(whole * whole, axis=0, keepdims=True)
-        for j in range(1, tp):
-            send(sums.at[t], sums.at[t], sum_send.at[1], sum_recv.at[1], {"tp": lax.rem(t + j, tp)})
+                send(back_copy, v_copy, copy_send, copy_recv, partner)
+                send(back_step, v_step, back_send[1], back_recv.at[1], partner)
+                send(back_new, v_new, back_send[1], back_recv.at[1], partner)
+
     with scope("masters_wait"):
         masters_end()
     with scope("mom_wait"):
-        landed(mom_top.at[pl.ds(0, fs - 1)], momt_recv.at[0])
-        landed(mom.at[pl.ds(0, fs - 1)], mom_recv.at[0])
+        landed(mom_top.at[pl.ds(0, fs - 1)], momt_recv)
+        landed(mom.at[pl.ds(0, fs - 1)], mom_recv)
         for i, whole in ((0, o1_all), (1, o2_all)):
             for g in range(fs):
                 whole[pl.ds(g * band, band), :] = decode_even(mom[g, i], mom_top[g, i])
-        left_here(mom_top.at[pl.ds(0, fs - 1)], momt_send.at[0])
-        left_here(mom.at[pl.ds(0, fs - 1)], mom_send.at[0])
-
+        left_here(mom_top.at[pl.ds(0, fs - 1)], momt_send)
+        left_here(mom.at[pl.ds(0, fs - 1)], mom_send)
+
+    n_sums = fs * chips
+    bands = o_all.at[pl.ds(0, (fs - 1) * band)]
     with scope("drain"):
-        copies = v_copy.at[pl.ds(0, (fs - 1) * v_rows)]
-
         @pl.when(aide)
         def _():
             left_here(heads_in, heads_send)
             left_here(ocot_in, ocot_send)
-            left_here(value_swap.at[pl.ds(0, fs - 1)], swap_send.at[2])
-            left_here(value_top.at[pl.ds(0, fs - 1)], mark_send.at[2])
-            left_here(value_momt.at[pl.ds(0, fs - 1)], momt_send.at[1])
-            left_here(value_mom.at[pl.ds(0, fs - 1)], mom_send.at[1])
-            left_here(value_sums.at[pl.ds(0, chips - 1)], sum_send.at[0])
+            left_here(value_swap.at[pl.ds(0, fs - 1)], value_swap_send)
+            left_here(value_top.at[pl.ds(0, fs - 1)], value_mark_send)
+            left_here(value_momt.at[pl.ds(0, fs - 1)], value_momt_send)
+            left_here(value_mom.at[pl.ds(0, fs - 1)], value_mom_send)
+            left_here(value_sums.at[pl.ds(0, chips - 1)], value_sum_send)
             for i in range(2):
-                left_here(mas.at[pl.ds(0, fs - 1)], mas_send.at[i])
-                left_here(mas_top.at[pl.ds(0, fs - 1)], mast_send.at[i])
-            left_here(v1_v, back_send.at[0])
-            left_here(vm_v, back_send.at[1])
-            left_here(v_copy.at[pl.ds(0, 2 * v_rows)], back_send.at[2])
+                left_here(mas.at[pl.ds(0, fs - 1)], mas_send[i])
+                left_here(mas_top.at[pl.ds(0, fs - 1)], mast_send[i])
+            left_here(v1_v, back_send[0])
+            left_here(vm_v, back_send[1])
+            left_here(v_copy, copy_send)
+            left_here(value_mast.at[pl.ds(0, fs - 1)], value_mast_send)
+            left_here(value_mas.at[pl.ds(0, fs - 1)], value_mas_send)
+            landed(o_all, all_recv)
+            landed(sums.at[pl.ds(0, n_sums)], sum_recv)
+
+        @pl.when(hub & (chip < last))
+        def _():
+            left_here(pre_out, pre_send)
+
+        @pl.when(hub & (chip > 0))
+        def _():
+            left_here(suf_out, suf_send)
 
         @pl.when(hub)
         def _():
@@ -533,29 +586,21 @@
                 left_here(ref.at[1], gift_send.at[i])
             left_here(pair_mast, give_send.at[0])
             left_here(pair_mas, give_send.at[1])
-            left_here(swap.at[pl.ds(0, fs - 1)], swap_send.at[0])
-            left_here(swap_top.at[pl.ds(0, fs - 1)], mark_send.at[0])
-            left_here(swap, swap_send.at[1])
-            left_here(swap_top, mark_send.at[1])
+            left_here(part_top_in.at[pl.ds(0, fs - 1)], mark_send)
+            left_here(part_in.at[pl.ds(0, fs - 1)], part_send)
             landed(v1_v, back_recv.at[0])
             landed(vm_v, back_recv.at[1])
-            left_here(copies, copy_send.at[0])
-            left_here(copies, copy_send.at[1])
-
-        @pl.when(hub & (chip < last))
-        def _():
-            left_here(pre_out, pre_send)
-
-        @pl.when(hub & (chip > 0))
-        def _():
-            left_here(suf_out, suf_send)
-
-    with scope("copy_wait"):
-        landed(copies, copy_recv)
-    with scope("sums_wait"):
-        landed(sums.at[pl.ds(0, tp - 1)], sum_recv.at[1])
-        totals[...] = jnp.sum(sums[...], axis=0)
-        left_here(sums.at[pl.ds(0, tp - 1)], sum_send.at[1])
+            with scope("copy_wait"):
+                landed(v_copy, copy_recv)
+            with scope("all_wait"):
+                landed(bands, all_recv)
+                left_here(bands, all_send.at[0])
+                left_here(o_all, all_send.at[1])
+            with scope("sums_wait"):
+                left_here(sums.at[pl.ds(0, 2 * n_sums - 1)], sum_send)
+                landed(sums.at[pl.ds(0, n_sums - 1)], sum_recv)
+
+    totals[...] = jnp.sum(sums[pl.ds(0, n_sums)], axis=0)
 
 
 def finish_kernel(
@@ -589,7 +634,8 @@
         return first_new, second_new
 
     own_band = pl.ds(pl.multiple_of(f * band, band), band)
-    first_v[...], second_v[...] = moments(o_all[own_band, :], om1[...], om2[...])
+    with jax.named_scope("f_own"):
+     first_v[...], second_v[...] = moments(o_all[own_band, :], om1[...], om2[...])
     put(first_v, o_first_out)
     put(second_v, o_second_out)
     first_new, second_new = moments(o_all[...], o1_all[...], o2_all[...])
@@ -601,8 +647,9 @@
 
     count = step_v.shape[0]
     own = pl.ds(pl.multiple_of(f * count, count), count)
-    move = step_of(own)
-    step_v[...] = move
+    with jax.named_scope("f_step"):
+        move = step_of(own)
+        step_v[...] = move
     put(step_v, o_step_out)
     new_v[...] = omas[...] - 0.002 * move
     put(new_v, o_new_out)
@@ -610,8 +657,9 @@
         rows = pl.ds(i * count, count)
         copy_v[rows, :] = (om_all[rows, :] - 0.002 * step_of(rows)).astype(BF16)
         put(copy_v.at[rows], o_copy_out.at[rows])
-    for copy in puts:
-        copy.wait()
+    with jax.named_scope("f_wait"):
+        for copy in puts:
+            copy.wait()
 
 
 def on_device(vin, vcot, vfac, vmas, vm1, vm2, heads, ocot, ofac, omas, om1, om2):
@@ -658,20 +706,21 @@
             wide(blocks, rank, block), wide(blocks, rank, block), wide(blocks, rank, block),
             coded(), coded(), coded(), coded(), wide(1, block),
             wide(2 * rank, columns), wide(2 * rank, columns),
-            pltpu.VMEM((rank, columns), BF16), wide(1, columns),
-            pltpu.VMEM((fs, rank, columns), BF16), wide(fs, 1, columns),
+            wide(2, rank, columns), pltpu.VMEM((fs, 2, band, columns), BF16), wide(2, 1, columns),
+            pltpu.VMEM((fs, 2, band, columns), BF16), wide(fs, 2, 1, columns), wide(band, columns),
             pltpu.VMEM((fs, 2, rank, columns), BF16), wide(fs, 2, 1, columns),
             wide(2, rank, columns),
             pltpu.VMEM((fs, 2, band, columns), BF16), wide(fs, 2, 1, columns),
-            pltpu.VMEM((fs, 2, 2, band, columns), BF16), wide(fs, 2, 2, 1, columns), wide(tp, 1, columns), wide(tp // 2, 1, columns),
+            pltpu.VMEM((fs, 2, 2, band, columns), BF16), wide(fs, 2, 2, 1, columns), wide(fs * tp, 1, columns), wide(tp // 2, 1, columns),
             pltpu.VMEM((fs, o_rows, columns), BF16), wide(fs, 1, columns),
             pltpu.VMEM((o_rows, columns), BF16), wide(1, columns),
             wide(band, columns), wide(band, columns), wide(v_rows, columns), wide(v_rows, columns),
-            pltpu.VMEM((v_rows, columns), BF16), pltpu.VMEM((v_rows, columns), BF16),
-            dma((10 + HEADS_PIECES,)), dma, dma((HEADS_PIECES,)), dma, dma, dma((4,)), dma((4,)),
+            pltpu.VMEM((fs * v_rows, columns), BF16),
+            pltpu.VMEM((fs, 2, v_rows, columns), BF16), wide(fs, 2, 1, columns), wide(fs * v_rows, columns),
+            dma((8 + len(growing(blocks)),)), dma((len(growing(blocks)),)), dma, dma((4,)),
             dma, dma((blocks,)), dma, dma((blocks,)),
-            dma((3,)), dma((2,)), dma((3,)), dma((2,)), dma((2,)), dma((2,)), pltpu.SemaphoreType.REGULAR((2,)),
-            dma((2,)), dma((2,)), dma((2,)), dma((2,)), dma((2,)), dma, dma((2,)), dma, dma((2,)), dma((2,)), dma((3,)), dma((3,)), dma((2,)), dma,
+            dma, dma, dma, dma, dma((2,)), dma, dma, dma, pltpu.SemaphoreType.REGULAR((2,)),
+            dma, dma, dma, dma, dma, dma, dma((2,)), dma((2,)), dma,
         ],
         compiler_params=pltpu.CompilerParams(
             collective_id=0, has_side_effects=True, vmem_limit_bytes=32 * 1024 * 1024

time: 30.5 us -> 29.2 us (0.957)
  Pallas kernels: 29.6 us -> 28.3 us
    pallas_call x1, Pallas kernels: 28.1 us -> 26.8 us  [on_device(): pl.pallas_call(functools.partial(gather_kernel, fs, tp), out_shape=(shape...]
where the time goes in v4:
time: 29.2 us; the launch traced here: 29 us
  Pallas kernels  28.3 us (97%)
  between operations  0.72 us (2%)
    pallas_call x1, Pallas kernels, on_device(): pl.pallas_call(functools.partial(gather_kernel, fs, tp), out_shape=(shape...  26.8 us
    pallas_call x1, Pallas kernels, on_device(): pl.pallas_call(functools.partial(finish_kernel, fs, tp), out_shape=(shape...  1.45 us

profile of v4, /device:TPU:0, one launch (start us, length us, event | category | flops | bytes accessed | tf_op | source)
XLA Modules:
  0.0 29.0 jit_solution(8130521014515253079)
XLA Ops:
  0.6 0.0 copy-start.3
  0.7 0.0 copy-start.2
  0.7 0.0 copy-start.1
  0.7 0.0 copy-start
  0.7 26.8 %shard_map.195 = (f32[128,256]{1,0:T(8,128)S(1)}, f32[128,256]{1,0:T(8,128)S(1)}, f32[128,256]{1,0:T(8,128)S(1)}, f32[1024,256]{1,0:T(8,128)S(1)}, f32[1,256]{1,...) custom-call(bf16[2048,256]{1,0:T(8,128)(2,1)} %vin.1, ...), custom_call_target="tpu_custom_call" | custom-call | tf_op jit(solution)/shard_map/pallas_call | solution.py:693
  27.5 0.0 copy-done.3
  27.5 0.0 copy-done.2
  27.5 0.0 copy-done.1
  27.6 0.0 copy-done
  27.6 1.5 %shard_map.196 = (f32[128,256]{1,0:T(8,128)}, f32[128,256]{1,0:T(8,128)}, bf16[512,256]{1,0:T(8,128)(2,1)}, f32[32,256]{1,0:T(8,128)}, f32[32,256]{1,0:T(8,128)}...) custom-call(f32[128,256]{1,0:T(8,128)S(1)} %get-tuple-element.20.o_a, ...), custom_call_target="tpu_custom_call" | custom-call | tf_op jit(solution)/shard_map/pallas_call | solution.py:733
Async XLA Ops:
  0.6 26.9 %copy-start.3 = (f32[32,256]{1,0:T(8,128)S(1)}, f32[32,256]{1,0:T(8,128)}, u32[]{:S(2)}) copy-start(f32[32,256]{1,0:T(8,128)} %om2.3) | copy-start | bytes 98308
  0.7 26.9 %copy-start.2 = (f32[32,256]{1,0:T(8,128)S(1)}, f32[32,256]{1,0:T(8,128)}, u32[]{:S(2)}) copy-start(f32[32,256]{1,0:T(8,128)} %om1.3) | copy-start | bytes 98308
  0.7 26.9 %copy-start.1 = (f32[256,256]{1,0:T(8,128)S(1)}, f32[256,256]{1,0:T(8,128)}, u32[]{:S(2)}) copy-start(f32[256,256]{1,0:T(8,128)} %omas.3) | copy-start | bytes 786436
  0.7 26.9 %copy-start = (bf16[1024,128]{1,0:T(8,128)(2,1)S(1)}, bf16[1024,128]{1,0:T(8,128)(2,1)}, u32[]{:S(2)}) copy-start(bf16[1024,128]{1,0:T(8,128)(2,1)} %ofac.3) | copy-start | bytes 786436

commit v5 on v4

--- a/solution.py
+++ b/solution.py
@@ -69,7 +69,7 @@
     o_all, o1_all, o2_all, om_all, totals, v_step, v_new, v_copy, v_first, v_second,
     vfac_v, ofac_v, vin_v, vcot_v, image_v, heads_v, heads_in, ocot_v, ocot_in, v1_v, v2_v, vm_v, om_v, o1_v, o2_v,
     own_v, left_v, right_v, pre_in, pre_out, suf_in, suf_out, bound, acc_own, acc_pair,
-    part, part_out, part_top, part_in, part_top_in, stage, value_swap, value_top, proj_v, mom, mom_top, value_mom, value_momt, sums, value_sums, mas, mas_top,
+    part, part_out, part_top, part_in, part_top_in, stage, value_out, value_top, value_in, value_top_in, proj_v, mom, mom_top, dir_code, dir_top, sums, value_sums, mas, mas_top,
     pair_mas, pair_mast, back_first, back_second, back_step, back_new, back_copy, value_mas, value_mast, move_v,
     load_sem, heads_recv, ocot_recv, gift_send, pre_send, pre_recv, suf_send, suf_recv,
     part_send, part_recv, mark_send, mark_recv, all_send, all_recv, sum_send, sum_recv, seen,
@@ -99,7 +99,7 @@
     gift_recv = [next(spare) for _ in range(4)]
     value_swap_send, value_swap_recv, value_mark_send, value_mark_recv = (next(spare) for _ in range(4))
     value_sum_send, value_sum_recv = next(spare), next(spare)
-    value_mom_send, value_mom_recv, value_momt_send, value_momt_recv = (next(spare) for _ in range(4))
+    dir_send, dir_recv, dirt_send, dirt_recv = (next(spare) for _ in range(4))
     mas_send, mast_send, give_recv = ([next(spare) for _ in range(2)] for _ in range(3))
     back_send = [next(spare) for _ in range(2)]
     copy_send = next(spare)
@@ -420,6 +420,9 @@
         with scope("value_load"):
             for load in (vfac_load, vcot_load, vin_load):
                 load.wait()
+        with scope("pass"):
+            pass_right((chip >= near) & (chip < last))
+            pass_left((chip > 0) & (chip < near))
         with scope("value_own"):
             total = jnp.zeros((2 * rank, columns), F32)
             stride = image_v.shape[2]
@@ -439,24 +442,24 @@
             totals_v.append(total)
             for h, total in enumerate(totals_v):
                 mine = total[:rank] + total[rank:]
+                proj_v[h] = mine
                 top = top_of(mine)
-                value_top[f, h] = top
-                value_swap[f, h] = encode_even(mine, top)
-            for d in fs_peers:
-                send(value_top.at[f], value_top.at[f], value_mark_send, value_mark_recv, {"fs": d})
-                send(value_swap.at[f], value_swap.at[f], value_swap_send, value_swap_recv, {"fs": d})
-        with scope("value_moments"):
-            vm12_load.wait()
-            landed(v1_v.at[1], gift_recv[1])
-            landed(v2_v.at[1], gift_recv[2])
-            for i, local in enumerate((v1_v, v2_v)):
-                for h in range(2):
-                    top = top_of(local[h])
-                    value_momt[f, i, h] = top
-                    value_mom[f, i, h] = encode_even(local[h], top)
-            for d in fs_peers:
-                send(value_momt.at[f], value_momt.at[f], value_momt_send, value_momt_recv, {"fs": d})
-                send(value_mom.at[f], value_mom.at[f], value_mom_send, value_mom_recv, {"fs": d})
+                value_top[h] = top
+                coded_part = encode_even(mine, top)
+                for g in range(fs):
+                    value_out[g, h] = coded_part[g * band:(g + 1) * band]
+        with scope("seen"):
+            @pl.when(chip == 0)
+            def _():
+                pl.semaphore_wait(seen.at[1], 1)
+
+            @pl.when(chip == last)
+            def _():
+                pl.semaphore_wait(seen.at[0], 1)
+
+        for d in fs_peers:
+            send(value_top, value_top_in.at[f], value_mark_send, value_mark_recv, {"fs": d})
+            send(value_out.at[d], value_in.at[f], value_swap_send, value_swap_recv, {"fs": d})
         with scope("give"):
             landed(pair_mast, give_recv[0])
             landed(pair_mas, give_recv[1])
@@ -471,60 +474,71 @@
                 top = top_of(vm_v[h])
                 value_mast[f, h] = top
                 value_mas[f, h] = encode_even(vm_v[h], top)
+        with scope("value_swap_wait"):
+            landed(value_top_in.at[pl.ds(0, fs - 1)], value_mark_recv)
+            landed(value_in.at[pl.ds(0, fs - 1)], value_swap_recv)
+        power = jnp.zeros((1, columns), F32)
+        own_band = pl.ds(pl.multiple_of(f * band, band), band)
+        for h in range(2):
+            whole = proj_v[h, own_band, :]
             for d in fs_peers:
-                send(value_mast.at[f], value_mast.at[f], value_mast_send, value_mast_recv, {"fs": d})
-                send(value_mas.at[f], value_mas.at[f], value_mas_send, value_mas_recv, {"fs": d})
-        pass_right((chip >= near) & (chip < last))
-        pass_left((chip > 0) & (chip < near))
-
-        @pl.when(chip == 0)
-        def _():
-            pl.semaphore_wait(seen.at[1], 1)
-
-        @pl.when(chip == last)
-        def _():
-            pl.semaphore_wait(seen.at[0], 1)
-
-        with scope("value_swap_wait"):
-            landed(value_top.at[pl.ds(0, fs - 1)], value_mark_recv)
-            landed(value_swap.at[pl.ds(0, fs - 1)], value_swap_recv)
-        power = jnp.zeros((1, columns), F32)
-        for h in range(2):
-            whole = decode_even(value_swap[0, h], value_top[0, h])
-            for g in range(1, fs):
-                whole = whole + decode_even(value_swap[g, h], value_top[g, h])
-            proj_v[h] = whole
+                whole = whole + decode_even(value_in[d, h], value_top_in[d, h])
+            proj_v[h, own_band, :] = whole
             power = power + jnp.sum(whole * whole, axis=0, keepdims=True)
-        value_sums[chip] = power
-        for j in range(1, chips):
-            where = {"tp": lax.rem(t + 2 * j, tp)}
-            send(value_sums.at[chip], value_sums.at[chip], value_sum_send, value_sum_recv, where)
+        value_me = f * chips + chip
+        value_sums[value_me] = power
+
+        def value_spread(i, j):
+            where = {"fs": lax.rem(f + i, fs), "tp": 2 * lax.rem(chip + j, chips)}
+            send(value_sums.at[value_me], value_sums.at[value_me], value_sum_send, value_sum_recv, where)
+
+        if fs * chips <= 16:
+            for i in range(fs - 1, -1, -1):
+                for j in range(chips):
+                    if (i, j) != (0, 0):
+                        value_spread(i, j)
+        else:
+            def value_spread_one(k, _):
+                value_spread(k // chips, k % chips)
+                return 0
+
+            lax.fori_loop(1, fs * chips, value_spread_one, 0)
+        for d in fs_peers:
+            send(value_mast.at[f], value_mast.at[f], value_mast_send, value_mast_recv, {"fs": d})
+            send(value_mas.at[f], value_mas.at[f], value_mas_send, value_mas_recv, {"fs": d})
+        vm12_load.wait()
+        landed(v1_v.at[1], gift_recv[1])
+        landed(v2_v.at[1], gift_recv[2])
         with scope("value_sums_wait"):
-            landed(value_sums.at[pl.ds(0, chips - 1)], value_sum_recv)
+            landed(value_sums.at[pl.ds(0, fs * chips - 1)], value_sum_recv)
         total = jnp.sum(jnp.sum(value_sums[...], axis=0), axis=1, keepdims=True)
         scale = lax.rsqrt(total / (rank * columns * tp) + 1e-06)
         for h, first_out, second_out in ((0, v_first, v_second), (1, back_first, back_second)):
-            scaled = scale * proj_v[h, pl.ds(pl.multiple_of(f * band, band), band), :]
-            first_out[...] = 0.9 * v1_v[h] + 0.1 * scaled
-            second_out[...] = 0.95 * v2_v[h] + 0.05 * scaled * scaled
+            scaled = scale * proj_v[h, own_band, :]
+            first_new = 0.9 * v1_v[h] + 0.1 * scaled
+            second_new = 0.95 * v2_v[h] + 0.05 * scaled * scaled
+            first_out[...] = first_new
+            second_out[...] = second_new
+            direction = first_new / (jnp.sqrt(second_new) + 1e-08)
+            top = top_of(direction)
+            dir_top[f, h] = top
+            dir_code[f, h] = encode_even(direction, top)
+        for d in fs_peers:
+            send(dir_top.at[f], dir_top.at[f], dirt_send, dirt_recv, {"fs": d})
+            send(dir_code.at[f], dir_code.at[f], dir_send, dir_recv, {"fs": d})
         send(back_first, v_first, back_send[0], back_recv.at[0], partner)
         send(back_second, v_second, back_send[0], back_recv.at[0], partner)
         rows = vfac_v[...]
         rows = jnp.concatenate([rows, rows], axis=1)
-        with scope("mom_wait"):
-            landed(value_momt.at[pl.ds(0, fs - 1)], value_momt_recv)
-            landed(value_mom.at[pl.ds(0, fs - 1)], value_mom_recv)
+        with scope("dir_wait"):
+            landed(dir_top.at[pl.ds(0, fs - 1)], dirt_recv)
+            landed(dir_code.at[pl.ds(0, fs - 1)], dir_recv)
             landed(value_mast.at[pl.ds(0, fs - 1)], value_mast_recv)
             landed(value_mas.at[pl.ds(0, fs - 1)], value_mas_recv)
 
-        def gathered(i, h):
-            return jnp.concatenate([decode_even(value_mom[g, i, h], value_momt[g, i, h]) for g in range(fs)], axis=0)
-
         for h, step_out, new_out, copy_out in ((1, back_step, back_new, back_copy), (0, v_step, v_new, v_copy)):
-            scaled = scale * proj_v[h]
-            first_new = 0.9 * gathered(0, h) + 0.1 * scaled
-            second_new = 0.95 * gathered(1, h) + 0.05 * scaled * scaled
-            direction = split(first_new / (jnp.sqrt(second_new) + 1e-08), 0)
+            direction = jnp.concatenate([decode_even(dir_code[g, h], dir_top[g, h]) for g in range(fs)], axis=0)
+            direction = split(direction, 0)
             move_v[...] = jnp.dot(rows, direction, preferred_element_type=F32)
             move = own_rows(move_v)[...]
             step_out[...] = move
@@ -556,11 +570,11 @@
         def _():
             left_here(heads_in, heads_send)
             left_here(ocot_in, ocot_send)
-            left_here(value_swap.at[pl.ds(0, fs - 1)], value_swap_send)
-            left_here(value_top.at[pl.ds(0, fs - 1)], value_mark_send)
-            left_here(value_momt.at[pl.ds(0, fs - 1)], value_momt_send)
-            left_here(value_mom.at[pl.ds(0, fs - 1)], value_mom_send)
-            left_here(value_sums.at[pl.ds(0, chips - 1)], value_sum_send)
+            left_here(value_in.at[pl.ds(0, fs - 1)], value_swap_send)
+            left_here(value_top_in.at[pl.ds(0, fs - 1)], value_mark_send)
+            left_here(dir_top.at[pl.ds(0, fs - 1)], dirt_send)
+            left_here(dir_code.at[pl.ds(0, fs - 1)], dir_send)
+            left_here(value_sums.at[pl.ds(0, n_sums - 1)], value_sum_send)
             for i in range(2):
                 left_here(mas.at[pl.ds(0, fs - 1)], mas_send[i])
                 left_here(mas_top.at[pl.ds(0, fs - 1)], mast_send[i])
@@ -708,10 +722,11 @@
             wide(2 * rank, columns), wide(2 * rank, columns),
             wide(2, rank, columns), pltpu.VMEM((fs, 2, band, columns), BF16), wide(2, 1, columns),
             pltpu.VMEM((fs, 2, band, columns), BF16), wide(fs, 2, 1, columns), wide(band, columns),
-            pltpu.VMEM((fs, 2, rank, columns), BF16), wide(fs, 2, 1, columns),
-            wide(2, rank, columns),
+            pltpu.VMEM((fs, 2, band, columns), BF16), wide(2, 1, columns),
+            pltpu.VMEM((fs, 2, band, columns), BF16), wide(fs, 2, 1, columns), wide(2, rank, columns),
             pltpu.VMEM((fs, 2, band, columns), BF16), wide(fs, 2, 1, columns),
-            pltpu.VMEM((fs, 2, 2, band, columns), BF16), wide(fs, 2, 2, 1, columns), wide(fs * tp, 1, columns), wide(tp // 2, 1, columns),
+            pltpu.VMEM((fs, 2, band, columns), BF16), wide(fs, 2, 1, columns),
+            wide(fs * tp, 1, columns), wide(fs * tp // 2, 1, columns),
             pltpu.VMEM((fs, o_rows, columns), BF16), wide(fs, 1, columns),
             pltpu.VMEM((o_rows, columns), BF16), wide(1, columns),
             wide(band, columns), wide(band, columns), wide(v_rows, columns), wide(v_rows, columns),

time: 29.2 us -> 28.9 us (0.990)
  no operation moved by 1% of the time
where the time goes in v5:
time: 28.9 us; the launch traced here: 28.8 us
  Pallas kernels  28.1 us (97%)
  between operations  0.72 us (2%)
    pallas_call x1, Pallas kernels, on_device(): pl.pallas_call(functools.partial(gather_kernel, fs, tp), out_shape=(shape...  26.6 us
    pallas_call x1, Pallas kernels, on_device(): pl.pallas_call(functools.partial(finish_kernel, fs, tp), out_shape=(shape...  1.45 us

profile of v5, /device:TPU:0, one launch (start us, length us, event | category | flops | bytes accessed | tf_op | source)
XLA Modules:
  0.0 28.8 jit_solution(13234066106324248192)
XLA Ops:
  0.6 0.0 copy-start.3
  0.7 0.0 copy-start.2
  0.7 0.0 copy-start.1
  0.7 0.0 copy-start
  0.7 26.6 %shard_map.195 = (f32[128,256]{1,0:T(8,128)S(1)}, f32[128,256]{1,0:T(8,128)S(1)}, f32[128,256]{1,0:T(8,128)S(1)}, f32[1024,256]{1,0:T(8,128)S(1)}, f32[1,256]{1,...) custom-call(bf16[2048,256]{1,0:T(8,128)(2,1)} %vin.1, ...), custom_call_target="tpu_custom_call" | custom-call | tf_op jit(solution)/shard_map/pallas_call | solution.py:707
  27.3 0.0 copy-done.3
  27.3 0.0 copy-done.2
  27.3 0.0 copy-done.1
  27.3 0.0 copy-done
  27.3 1.4 %shard_map.196 = (f32[128,256]{1,0:T(8,128)}, f32[128,256]{1,0:T(8,128)}, bf16[512,256]{1,0:T(8,128)(2,1)}, f32[32,256]{1,0:T(8,128)}, f32[32,256]{1,0:T(8,128)}...) custom-call(f32[128,256]{1,0:T(8,128)S(1)} %get-tuple-element.20.o_a, ...), custom_call_target="tpu_custom_call" | custom-call | tf_op jit(solution)/shard_map/pallas_call | solution.py:748
Async XLA Ops:
  0.6 26.7 %copy-start.3 = (f32[32,256]{1,0:T(8,128)S(1)}, f32[32,256]{1,0:T(8,128)}, u32[]{:S(2)}) copy-start(f32[32,256]{1,0:T(8,128)} %om2.3) | copy-start | bytes 98308
  0.7 26.7 %copy-start.2 = (f32[32,256]{1,0:T(8,128)S(1)}, f32[32,256]{1,0:T(8,128)}, u32[]{:S(2)}) copy-start(f32[32,256]{1,0:T(8,128)} %om1.3) | copy-start | bytes 98308
  0.7 26.7 %copy-start.1 = (f32[256,256]{1,0:T(8,128)S(1)}, f32[256,256]{1,0:T(8,128)}, u32[]{:S(2)}) copy-start(f32[256,256]{1,0:T(8,128)} %omas.3) | copy-start | bytes 786436
  0.7 26.7 %copy-start = (bf16[1024,128]{1,0:T(8,128)(2,1)S(1)}, bf16[1024,128]{1,0:T(8,128)(2,1)}, u32[]{:S(2)}) copy-start(bf16[1024,128]{1,0:T(8,128)(2,1)} %ofac.3) | copy-start | bytes 786436

commit v6 on v5

--- a/solution.py
+++ b/solution.py
@@ -15,7 +15,7 @@
 F32 = jnp.float32
 PRE = 6
 SUF = 7
-LEVELS = 252.0
+LEVELS = 250.0
 POWER = 7
 PEAK = 240000.0
 HEADS_BOUND = 6.0
@@ -48,7 +48,8 @@
 
 def decode_even(coded, top):
     y = coded.astype(F32)
-    size = (jnp.log2(jnp.maximum(jnp.abs(y), 1e-38)) + LEVELS / 2) * (top * (1.0 / LEVELS))
+    level = jnp.maximum(jnp.log2(jnp.maximum(jnp.abs(y), 1e-38)) + LEVELS / 2, 0.0)
+    size = level * (top * (1.0 / LEVELS))
     return jnp.where(y < 0.0, -size, size)
 
 
@@ -70,7 +71,7 @@
     vfac_v, ofac_v, vin_v, vcot_v, image_v, heads_v, heads_in, ocot_v, ocot_in, v1_v, v2_v, vm_v, om_v, o1_v, o2_v,
     own_v, left_v, right_v, pre_in, pre_out, suf_in, suf_out, bound, acc_own, acc_pair,
     part, part_out, part_top, part_in, part_top_in, stage, value_out, value_top, value_in, value_top_in, proj_v, mom, mom_top, dir_code, dir_top, sums, value_sums, mas, mas_top,
-    pair_mas, pair_mast, back_first, back_second, back_step, back_new, back_copy, value_mas, value_mast, move_v,
+    back_first, back_second, back_step, back_new, back_copy, value_mas, value_mast, move_v,
     load_sem, heads_recv, ocot_recv, gift_send, pre_send, pre_recv, suf_send, suf_recv,
     part_send, part_recv, mark_send, mark_recv, all_send, all_recv, sum_send, sum_recv, seen,
     mom_send, mom_recv, momt_send, momt_recv, mas_recv, mast_recv, give_send, back_recv, copy_recv,
@@ -94,13 +95,13 @@
     at_last = (last - chip + last) // chips
     at_first = (chip + last) // chips
 
-    spare = iter([sems.at[i] for sems in (pre_recv, suf_recv) for i in range(blocks)])
+    spare = iter([sems.at[i] for sems in (pre_recv, suf_recv, heads_recv) for i in range(sems.shape[0])])
     heads_send, ocot_send = next(spare), next(spare)
     gift_recv = [next(spare) for _ in range(4)]
     value_swap_send, value_swap_recv, value_mark_send, value_mark_recv = (next(spare) for _ in range(4))
     value_sum_send, value_sum_recv = next(spare), next(spare)
     dir_send, dir_recv, dirt_send, dirt_recv = (next(spare) for _ in range(4))
-    mas_send, mast_send, give_recv = ([next(spare) for _ in range(2)] for _ in range(3))
+    mas_send, mast_send = next(spare), next(spare)
     back_send = [next(spare) for _ in range(2)]
     copy_send = next(spare)
     value_mas_send, value_mas_recv, value_mast_send, value_mast_recv = (next(spare) for _ in range(4))
@@ -126,16 +127,17 @@
     om1_load = loading(count, om1, o1_v)
     om2_load = loading(count, om2, o2_v)
     om12_load = loading(count, om_v.at[pl.ds(0, 2 * band)], om_v.at[pl.ds(0, 2 * band)])
-    omas_load = loading(count + 2, omas, om_v)
-    ocot_load = loading(count + 3, ocot, ocot_v)
-    ofac_load = loading(count + 4, ofac, ofac_v)
-    vfac_load = loading(count + 4, vfac, vfac_v)
-    vcot_load = loading(count + 5, vcot, vcot_v)
-    vin_load = loading(count + 6, vin, vin_v.at[0])
-    vm1_load = loading(count + 1, vm1, v1_v.at[0])
-    vm2_load = loading(count + 1, vm2, v2_v.at[0])
-    vm12_load = loading(count + 1, v1_v, v1_v)
-    vmas_load = loading(count + 7, vmas, vm_v.at[0])
+    omas_load = loading(count + 1, omas, om_v)
+    ocot_load = loading(count + 2, ocot, ocot_v)
+    ofac_load = loading(count + 3, ofac, ofac_v)
+    vfac_load = pltpu.make_async_copy(vfac, vfac_v, next(spare))
+    vcot_load = pltpu.make_async_copy(vcot, vcot_v, next(spare))
+    vin_load = pltpu.make_async_copy(vin, vin_v.at[0], next(spare))
+    vmas_load = pltpu.make_async_copy(vmas, vm_v.at[0], next(spare))
+    moments_sem = next(spare)
+    vm1_load = pltpu.make_async_copy(vm1, v1_v.at[0], moments_sem)
+    vm2_load = pltpu.make_async_copy(vm2, v2_v.at[0], moments_sem)
+    vm12_load = pltpu.make_async_copy(v1_v, v1_v, moments_sem)
 
     heads_load[0].start()
 
@@ -293,7 +295,7 @@
     @pl.when(hub)
     def _():
         for i, (src, dst) in enumerate(((vin, vin_v), (vm1, v1_v), (vm2, v2_v), (vmas, vm_v))):
-            send(src, dst.at[1], gift_send.at[i], gift_recv[i], partner)
+            send(src, dst.at[1], gift_send.at[min(i, 1)], gift_recv[i], partner)
         send_moments()
         with scope("factor"):
             ofac_load.wait()
@@ -334,15 +336,18 @@
         acc_pair[...] = jnp.zeros_like(acc_pair)
         with scope("masters_encode"):
             masters_encode()
-        send(mas_top.at[f], pair_mast, give_send.at[0], give_recv[0], partner)
-        send(mas.at[f], pair_mas, give_send.at[1], give_recv[1], partner)
+
+        def hub_masters():
+            for d in fs_peers:
+                send(mas_top.at[f], mas_top.at[f], give_send.at[0], mast_recv, {"fs": d})
+                send(mas.at[f], mas.at[f], give_send.at[1], mas_recv, {"fs": d})
 
         def output_cotangents():
             ocot_load.wait()
             landed(ocot_in, ocot_recv)
 
         done = 0
-        for at, event in ((13, output_cotangents),):
+        for at, event in ((13, output_cotangents), (22, hub_masters)):
             at = min(at, steps)
             lax.fori_loop(done, at, step, 0)
             done = at
@@ -377,22 +382,22 @@
             me = f * chips + chip
             sums[me] = power
 
-            def spread(i, j, c):
-                where = {"fs": lax.rem(f + i, fs), "tp": 2 * lax.rem(chip + j, chips) + c}
+            def spread(d, j, c):
+                where = {"fs": d, "tp": 2 * lax.rem(chip + j, chips) + c}
                 send(sums.at[me], sums.at[me], sum_send, sum_recv, where)
 
             if fs * chips <= 16:
-                for i in range(fs - 1, -1, -1):
-                    for j in range(chips):
+                for j in range(chips - 1, -1, -1):
+                    for d in (*fs_peers, f):
                         for c in range(2):
-                            if (i, j, c) != (0, 0, 1):
-                                spread(i, j, c)
+                            if d is not f or j > 0 or c == 0:
+                                spread(d, j, c)
             else:
                 def spread_one(k, _):
-                    spread(k // (2 * chips), (k // 2) % chips, k % 2)
+                    spread(lax.rem(f + k // (2 * chips), fs), (k // 2) % chips, k % 2)
                     return 0
 
-                spread(0, 0, 0)
+                spread(f, 0, 0)
                 lax.fori_loop(2, 2 * fs * chips, spread_one, 0)
             here = own_rows(o_all)
             for d in fs_peers:
@@ -411,8 +416,8 @@
         with scope("masters_encode"):
             masters_encode()
         for d in fs_peers:
-            send(mas_top.at[f], mas_top.at[f], mast_send[0], mast_recv, {"fs": d})
-            send(mas.at[f], mas.at[f], mas_send[0], mas_recv, {"fs": d})
+            send(mas_top.at[f], mas_top.at[f], mast_send, mast_recv, {"fs": d})
+            send(mas.at[f], mas.at[f], mas_send, mas_recv, {"fs": d})
         ocot_load.wait()
         send(ocot_v, ocot_in, ocot_send, ocot_recv, partner)
         pass_right((chip > 0) & (chip < near))
@@ -460,13 +465,6 @@
         for d in fs_peers:
             send(value_top, value_top_in.at[f], value_mark_send, value_mark_recv, {"fs": d})
             send(value_out.at[d], value_in.at[f], value_swap_send, value_swap_recv, {"fs": d})
-        with scope("give"):
-            landed(pair_mast, give_recv[0])
-            landed(pair_mas, give_recv[1])
-        for d in fs_peers:
-            there = {"fs": d, "tp": t + 1}
-            send(pair_mast, mas_top.at[f], mast_send[1], mast_recv, there)
-            send(pair_mas, mas.at[f], mas_send[1], mas_recv, there)
         with scope("value_masters"):
             vmas_load.wait()
             landed(vm_v.at[1], gift_recv[3])
@@ -474,6 +472,9 @@
                 top = top_of(vm_v[h])
                 value_mast[f, h] = top
                 value_mas[f, h] = encode_even(vm_v[h], top)
+            for d in fs_peers:
+                send(value_mast.at[f], value_mast.at[f], value_mast_send, value_mast_recv, {"fs": d})
+                send(value_mas.at[f], value_mas.at[f], value_mas_send, value_mas_recv, {"fs": d})
         with scope("value_swap_wait"):
             landed(value_top_in.at[pl.ds(0, fs - 1)], value_mark_recv)
             landed(value_in.at[pl.ds(0, fs - 1)], value_swap_recv)
@@ -503,9 +504,6 @@
                 return 0
 
             lax.fori_loop(1, fs * chips, value_spread_one, 0)
-        for d in fs_peers:
-            send(value_mast.at[f], value_mast.at[f], value_mast_send, value_mast_recv, {"fs": d})
-            send(value_mas.at[f], value_mas.at[f], value_mas_send, value_mas_recv, {"fs": d})
         vm12_load.wait()
         landed(v1_v.at[1], gift_recv[1])
         landed(v2_v.at[1], gift_recv[2])
@@ -526,8 +524,8 @@
         for d in fs_peers:
             send(dir_top.at[f], dir_top.at[f], dirt_send, dirt_recv, {"fs": d})
             send(dir_code.at[f], dir_code.at[f], dir_send, dir_recv, {"fs": d})
-        send(back_first, v_first, back_send[0], back_recv.at[0], partner)
-        send(back_second, v_second, back_send[0], back_recv.at[0], partner)
+        send(back_first, v_first, back_send[0], back_recv, partner)
+        send(back_second, v_second, back_send[0], back_recv, partner)
         rows = vfac_v[...]
         rows = jnp.concatenate([rows, rows], axis=1)
         with scope("dir_wait"):
@@ -549,8 +547,8 @@
                 copy_out[these, :] = (old - 0.002 * move_v[these, :]).astype(BF16)
             if h == 1:
                 send(back_copy, v_copy, copy_send, copy_recv, partner)
-                send(back_step, v_step, back_send[1], back_recv.at[1], partner)
-                send(back_new, v_new, back_send[1], back_recv.at[1], partner)
+                send(back_step, v_step, back_send[1], back_recv, partner)
+                send(back_new, v_new, back_send[1], back_recv, partner)
 
     with scope("masters_wait"):
         masters_end()
@@ -575,9 +573,8 @@
             left_here(dir_top.at[pl.ds(0, fs - 1)], dirt_send)
             left_here(dir_code.at[pl.ds(0, fs - 1)], dir_send)
             left_here(value_sums.at[pl.ds(0, n_sums - 1)], value_sum_send)
-            for i in range(2):
-                left_here(mas.at[pl.ds(0, fs - 1)], mas_send[i])
-                left_here(mas_top.at[pl.ds(0, fs - 1)], mast_send[i])
+            left_here(mas.at[pl.ds(0, fs - 1)], mas_send)
+            left_here(mas_top.at[pl.ds(0, fs - 1)], mast_send)
             left_here(v1_v, back_send[0])
             left_here(vm_v, back_send[1])
             left_here(v_copy, copy_send)
@@ -596,14 +593,13 @@
 
         @pl.when(hub)
         def _():
-            for i, ref in enumerate((vin_v, v1_v, v2_v, vm_v)):
-                left_here(ref.at[1], gift_send.at[i])
-            left_here(pair_mast, give_send.at[0])
-            left_here(pair_mas, give_send.at[1])
+            left_here(vin_v.at[1], gift_send.at[0])
+            left_here(om_v.at[pl.ds(0, 2 * band + v_rows)], gift_send.at[1])
+            left_here(mas_top.at[pl.ds(0, fs - 1)], give_send.at[0])
+            left_here(mas.at[pl.ds(0, fs - 1)], give_send.at[1])
             left_here(part_top_in.at[pl.ds(0, fs - 1)], mark_send)
             left_here(part_in.at[pl.ds(0, fs - 1)], part_send)
-            landed(v1_v, back_recv.at[0])
-            landed(vm_v, back_recv.at[1])
+            landed(om_all.at[pl.ds(0, 2 * (band + v_rows))], back_recv)
             with scope("copy_wait"):
                 landed(v_copy, copy_recv)
             with scope("all_wait"):
@@ -622,7 +618,7 @@
     o_all, o1_all, o2_all, om_all, totals, ofac, omas, om1, om2, v_step, v_new, v_copy, v_first, v_second,
     v_step_out, v_new_out, v_copy_out, v_first_out, v_second_out,
     o_step_out, o_new_out, o_copy_out, o_first_out, o_second_out,
-    step_v, new_v, copy_v, first_v, second_v, out_sem,
+    move_v, new_v, copy_v, first_v, second_v, out_sem,
 ):
     f = lax.axis_index("fs")
     puts = []
@@ -659,18 +655,16 @@
         left = ofac[rows, :]
         return jnp.dot(jnp.concatenate([left, left], axis=1), direction, preferred_element_type=F32)
 
-    count = step_v.shape[0]
-    own = pl.ds(pl.multiple_of(f * count, count), count)
-    with jax.named_scope("f_step"):
-        move = step_of(own)
-        step_v[...] = move
-    put(step_v, o_step_out)
-    new_v[...] = omas[...] - 0.002 * move
-    put(new_v, o_new_out)
+    count = new_v.shape[0]
     for i in range(fs):
         rows = pl.ds(i * count, count)
-        copy_v[rows, :] = (om_all[rows, :] - 0.002 * step_of(rows)).astype(BF16)
+        move_v[rows, :] = step_of(rows)
+        copy_v[rows, :] = (om_all[rows, :] - 0.002 * move_v[rows, :]).astype(BF16)
         put(copy_v.at[rows], o_copy_out.at[rows])
+    own = pl.ds(pl.multiple_of(f * count, count), count)
+    put(move_v.at[own], o_step_out)
+    new_v[...] = omas[...] - 0.002 * move_v[own, :]
+    put(new_v, o_new_out)
     with jax.named_scope("f_wait"):
         for copy in puts:
             copy.wait()
@@ -728,14 +722,13 @@
             pltpu.VMEM((fs, 2, band, columns), BF16), wide(fs, 2, 1, columns),
             wide(fs * tp, 1, columns), wide(fs * tp // 2, 1, columns),
             pltpu.VMEM((fs, o_rows, columns), BF16), wide(fs, 1, columns),
-            pltpu.VMEM((o_rows, columns), BF16), wide(1, columns),
             wide(band, columns), wide(band, columns), wide(v_rows, columns), wide(v_rows, columns),
             pltpu.VMEM((fs * v_rows, columns), BF16),
             pltpu.VMEM((fs, 2, v_rows, columns), BF16), wide(fs, 2, 1, columns), wide(fs * v_rows, columns),
-            dma((8 + len(growing(blocks)),)), dma((len(growing(blocks)),)), dma, dma((4,)),
+            dma((4 + len(growing(blocks)),)), dma((len(growing(blocks)),)), dma, dma((2,)),
             dma, dma((blocks,)), dma, dma((blocks,)),
             dma, dma, dma, dma, dma((2,)), dma, dma, dma, pltpu.SemaphoreType.REGULAR((2,)),
-            dma, dma, dma, dma, dma, dma, dma((2,)), dma((2,)), dma,
+            dma, dma, dma, dma, dma, dma, dma((2,)), dma, dma,
         ],
         compiler_params=pltpu.CompilerParams(
             collective_id=0, has_side_effects=True, vmem_limit_bytes=32 * 1024 * 1024
@@ -756,7 +749,7 @@
         in_specs=[VMEM] * 14,
         out_specs=(HBM,) * 10,
         scratch_shapes=[
-            wide(o_rows, columns), wide(o_rows, columns), pltpu.VMEM((fs * o_rows, columns), BF16),
+            wide(fs * o_rows, columns), wide(o_rows, columns), pltpu.VMEM((fs * o_rows, columns), BF16),
             wide(band, columns), wide(band, columns), dma((9 + fs,)),
         ],
         compiler_params=pltpu.CompilerParams(vmem_limit_bytes=24 * 1024 * 1024),

time: 28.9 us -> 29 us (level)
  no operation moved by 1% of the time
where the time goes in v6:
time: 29 us; the launch traced here: 28.9 us
  Pallas kernels  28.2 us (97%)
  between operations  0.72 us (2%)
    pallas_call x1, Pallas kernels, on_device(): pl.pallas_call(functools.partial(gather_kernel, fs, tp), out_shape=(shape...  26.6 us
    pallas_call x1, Pallas kernels, on_device(): pl.pallas_call(functools.partial(finish_kernel, fs, tp), out_shape=(shape...  1.58 us

profile of v6, /device:TPU:0, one launch (start us, length us, event | category | flops | bytes accessed | tf_op | source)
XLA Modules:
  0.0 28.9 jit_solution(5423577589404460269)
XLA Ops:
  0.6 0.0 copy-start.3
  0.7 0.0 copy-start.2
  0.7 0.0 copy-start.1
  0.7 0.0 copy-start
  0.7 26.6 %shard_map.195 = (f32[128,256]{1,0:T(8,128)S(1)}, f32[128,256]{1,0:T(8,128)S(1)}, f32[128,256]{1,0:T(8,128)S(1)}, f32[1024,256]{1,0:T(8,128)S(1)}, f32[1,256]{1,...) custom-call(bf16[2048,256]{1,0:T(8,128)(2,1)} %vin.1, ...), custom_call_target="tpu_custom_call" | custom-call | tf_op jit(solution)/shard_map/pallas_call | solution.py:701
  27.3 0.0 copy-done.3
  27.3 0.0 copy-done.2
  27.3 0.0 copy-done.1
  27.3 0.0 copy-done
  27.3 1.6 %shard_map.196 = (f32[128,256]{1,0:T(8,128)}, f32[128,256]{1,0:T(8,128)}, bf16[512,256]{1,0:T(8,128)(2,1)}, f32[32,256]{1,0:T(8,128)}, f32[32,256]{1,0:T(8,128)}...) custom-call(f32[128,256]{1,0:T(8,128)S(1)} %get-tuple-element.20.o_a, ...), custom_call_target="tpu_custom_call" | custom-call | tf_op jit(solution)/shard_map/pallas_call | solution.py:741
Async XLA Ops:
  0.6 26.6 %copy-start.3 = (f32[32,256]{1,0:T(8,128)S(1)}, f32[32,256]{1,0:T(8,128)}, u32[]{:S(2)}) copy-start(f32[32,256]{1,0:T(8,128)} %om2.3) | copy-start | bytes 98308
  0.7 26.6 %copy-start.2 = (f32[32,256]{1,0:T(8,128)S(1)}, f32[32,256]{1,0:T(8,128)}, u32[]{:S(2)}) copy-start(f32[32,256]{1,0:T(8,128)} %om1.3) | copy-start | bytes 98308
  0.7 26.6 %copy-start.1 = (f32[256,256]{1,0:T(8,128)S(1)}, f32[256,256]{1,0:T(8,128)}, u32[]{:S(2)}) copy-start(f32[256,256]{1,0:T(8,128)} %omas.3) | copy-start | bytes 786436
  0.7 26.6 %copy-start = (bf16[1024,128]{1,0:T(8,128)(2,1)S(1)}, bf16[1024,128]{1,0:T(8,128)(2,1)}, u32[]{:S(2)}) copy-start(bf16[1024,128]{1,0:T(8,128)(2,1)} %ofac.3) | copy-start | bytes 786436

commit v7 on v5

--- a/solution.py
+++ b/solution.py
@@ -15,7 +15,7 @@
 F32 = jnp.float32
 PRE = 6
 SUF = 7
-LEVELS = 252.0
+LEVELS = 250.0
 POWER = 7
 PEAK = 240000.0
 HEADS_BOUND = 6.0
@@ -48,7 +48,8 @@
 
 def decode_even(coded, top):
     y = coded.astype(F32)
-    size = (jnp.log2(jnp.maximum(jnp.abs(y), 1e-38)) + LEVELS / 2) * (top * (1.0 / LEVELS))
+    level = jnp.maximum(jnp.log2(jnp.maximum(jnp.abs(y), 1e-38)) + LEVELS / 2, 0.0)
+    size = level * (top * (1.0 / LEVELS))
     return jnp.where(y < 0.0, -size, size)
 
 

time: 28.9 us -> 29 us (level)
  no operation moved by 1% of the time
where the time goes in v7:
time: 29 us; the launch traced here: 28.8 us
  Pallas kernels  28.1 us (97%)
  between operations  0.72 us (2%)
    pallas_call x1, Pallas kernels, on_device(): pl.pallas_call(functools.partial(gather_kernel, fs, tp), out_shape=(shape...  26.6 us
    pallas_call x1, Pallas kernels, on_device(): pl.pallas_call(functools.partial(finish_kernel, fs, tp), out_shape=(shape...  1.45 us

profile of v7, /device:TPU:0, one launch (start us, length us, event | category | flops | bytes accessed | tf_op | source)
XLA Modules:
  0.0 28.8 jit_solution(4454733525761951887)
XLA Ops:
  0.6 0.0 copy-start.3
  0.7 0.0 copy-start.2
  0.7 0.0 copy-start.1
  0.7 0.0 copy-start
  0.7 26.6 %shard_map.195 = (f32[128,256]{1,0:T(8,128)S(1)}, f32[128,256]{1,0:T(8,128)S(1)}, f32[128,256]{1,0:T(8,128)S(1)}, f32[1024,256]{1,0:T(8,128)S(1)}, f32[1,256]{1,...) custom-call(bf16[2048,256]{1,0:T(8,128)(2,1)} %vin.1, ...), custom_call_target="tpu_custom_call" | custom-call | tf_op jit(solution)/shard_map/pallas_call | solution.py:708
  27.3 0.0 copy-done.3
  27.3 0.0 copy-done.2
  27.3 0.0 copy-done.1
  27.3 0.0 copy-done
  27.3 1.5 %shard_map.196 = (f32[128,256]{1,0:T(8,128)}, f32[128,256]{1,0:T(8,128)}, bf16[512,256]{1,0:T(8,128)(2,1)}, f32[32,256]{1,0:T(8,128)}, f32[32,256]{1,0:T(8,128)}...) custom-call(f32[128,256]{1,0:T(8,128)S(1)} %get-tuple-element.20.o_a, ...), custom_call_target="tpu_custom_call" | custom-call | tf_op jit(solution)/shard_map/pallas_call | solution.py:749
Async XLA Ops:
  0.6 26.7 %copy-start.3 = (f32[32,256]{1,0:T(8,128)S(1)}, f32[32,256]{1,0:T(8,128)}, u32[]{:S(2)}) copy-start(f32[32,256]{1,0:T(8,128)} %om2.3) | copy-start | bytes 98308
  0.7 26.7 %copy-start.2 = (f32[32,256]{1,0:T(8,128)S(1)}, f32[32,256]{1,0:T(8,128)}, u32[]{:S(2)}) copy-start(f32[32,256]{1,0:T(8,128)} %om1.3) | copy-start | bytes 98308
  0.7 26.7 %copy-start.1 = (f32[256,256]{1,0:T(8,128)S(1)}, f32[256,256]{1,0:T(8,128)}, u32[]{:S(2)}) copy-start(f32[256,256]{1,0:T(8,128)} %omas.3) | copy-start | bytes 786436
  0.7 26.7 %copy-start = (bf16[1024,128]{1,0:T(8,128)(2,1)S(1)}, bf16[1024,128]{1,0:T(8,128)(2,1)}, u32[]{:S(2)}) copy-start(bf16[1024,128]{1,0:T(8,128)(2,1)} %ofac.3) | copy-start | bytes 786436
